TPU v7x, 32 devices: a whole 2x2x4 slice. The times are simulated.
32 devices in a mesh: sp: 8 (over z, x), tp: 4 (over y, core).
Axes of the slice: x: 2, y: 2, z: 4, core: 2. Of those that a mesh axis runs over, the one named last changes fastest.
Arguments:
- out_cotangent: bfloat16 [2048, 2048], P('sp'), may hold values from -6 to 6
- stream: bfloat16 [2048, 2048], P('sp'), may hold values from -6 to 6
- route_ids: int32 [2048, 2], P('sp'), may hold values from 0 to 7, all different within a row; in each aligned block of 256 rows (0 to 255, 256 to 511, ...) at most 128 rows name the same one
- route_weights: float32 [2048, 2], P('sp'), may hold values from 0.3 to 2
- gate_proj: bfloat16 [8, 2048, 1024], P('sp', None, 'tp'), may hold values from -0.125 to 0.125
- up_proj: bfloat16 [8, 2048, 1024], P('sp', None, 'tp'), may hold values from -0.125 to 0.125
- down_proj: bfloat16 [8, 1024, 2048], P('sp', 'tp'), may hold values from -0.1875 to 0.1875
- outer_gate: bfloat16 [2048, 512], P('sp', 'tp'), may hold values from -6 to 6
- inner_gate: bfloat16 [2048, 512], P('sp', 'tp'), may hold values from -6 to 6
- conv_input: bfloat16 [2048, 512], P('sp', 'tp'), may hold values from -6 to 6
- conv_taps: float32 [3, 512], P(None, 'tp'), may hold values from -4 to 4
- out_proj: bfloat16 [2048, 512], P(None, 'tp'), may hold values from -0.25 to 0.25
Outputs:
- grad_gate_proj: bfloat16 [8, 2048, 1024], P('sp', None, 'tp')
- grad_up_proj: bfloat16 [8, 2048, 1024], P('sp', None, 'tp')
- grad_down_proj: bfloat16 [8, 1024, 2048], P('sp', 'tp')
- grad_out_proj: float32 [2048, 512], P('sp', 'tp')
- grad_outer_gate: float32 [2048, 512], P('sp', 'tp')
- grad_inner_gate: float32 [2048, 512], P('sp', 'tp')
- grad_conv_input: float32 [2048, 512], P('sp', 'tp')
Inputs may be any that keep to these rules, and one draw needn't show every extreme that they name: `route_ids`: the 2 experts of a token differ. Among the tokens of one index of sp, no expert is chosen more than 128 times, and in every draw some expert is chosen exactly 128 times by them.
All inputs are finite; a program needn't handle non-finite values.
Results may differ from a plain program's by a relative error of at most 0.018.
Values may be sent and summed in bfloat16 or wider, within the bound.
A program may use at most 64 MiB of HBM per device.

v0:
```python
import jax
import jax.numpy as jnp
from jax import lax
from jax.sharding import PartitionSpec as P


def passed_along(x, axis, by):
    devices = lax.axis_size(axis)
    pairs = [(i, i + by) for i in range(devices) if 0 <= i + by < devices]
    return lax.ppermute(x, axis, pairs)


def to_owners(x, devices):
    blocks = x.reshape(devices, -1, x.shape[1])
    return lax.all_to_all(blocks, "sp", split_axis=0, concat_axis=0, tiled=True).reshape(x.shape)


def partial_rows(d_gate, d_up, w_gate, w_up):
    across = (((1,), (1,)), ((), ()))
    total = lax.dot_general(
        d_gate, w_gate, across, preferred_element_type=jnp.float32
    ) + lax.dot_general(d_up, w_up, across, preferred_element_type=jnp.float32)
    return total.astype(jnp.bfloat16)


def reduced_quarter(d_gate, d_up, w_gate, w_up):
    devices = lax.axis_size("tp")
    if devices != 4:
        return lax.psum_scatter(
            partial_rows(d_gate, d_up, w_gate, w_up), "tp", scatter_dimension=1, tiled=True
        )
    quarter = w_gate.shape[0] // devices
    me = lax.axis_index("tp")

    def rows_of(w, *flips):
        return jnp.concatenate(
            [lax.dynamic_slice_in_dim(w, (me ^ flip) * quarter, quarter, 0) for flip in flips]
        )

    def swapped(x, flip):
        return lax.ppermute(x, "tp", [(i, i ^ flip) for i in range(devices)])

    sent = partial_rows(d_gate, d_up, rows_of(w_gate, 1, 3), rows_of(w_up, 1, 3))
    got = swapped(sent, 1)
    kept = partial_rows(d_gate, d_up, rows_of(w_gate, 0, 2), rows_of(w_up, 0, 2))
    far = kept[:, quarter:].astype(jnp.float32) + got[:, quarter:].astype(jnp.float32)
    near = kept[:, :quarter].astype(jnp.float32) + got[:, :quarter].astype(jnp.float32)
    other = swapped(far.astype(jnp.bfloat16), 2)
    return (near + other.astype(jnp.float32)).astype(jnp.bfloat16)


def shards(
    out_cotangent,
    stream,
    route_ids,
    route_weights,
    gate_proj,
    up_proj,
    down_proj,
    outer_gate,
    inner_gate,
    conv_input,
    conv_taps,
    out_proj,
):
    sp_devices = lax.axis_size("sp")
    tokens_here, width = stream.shape
    experts = sp_devices * gate_proj.shape[0]
    capacity = 4 * tokens_here // experts
    quarter = width // lax.axis_size("tp")
    first_column = lax.axis_index("tp") * quarter
    own_cotangent = lax.dynamic_slice_in_dim(out_cotangent, first_column, quarter, 1)
    own_stream = lax.dynamic_slice_in_dim(stream, first_column, quarter, 1)
    over_rows = (((0,), (0,)), ((), ()))
    expert_ids = jnp.arange(experts, dtype=jnp.int32)
    chosen = route_ids[:, :, None] == expert_ids
    hit = jnp.any(chosen, axis=1)
    token_weight = jnp.sum(jnp.where(chosen, route_weights[:, :, None], 0.0), axis=1)
    token_ids = jnp.arange(tokens_here, dtype=jnp.int32)
    below = (token_ids[:, None] < token_ids[None, :]).astype(jnp.bfloat16)
    rank = lax.dot_general(
        hit.astype(jnp.bfloat16), below, over_rows, preferred_element_type=jnp.float32
    )
    rank = jnp.where(hit.T, rank, -1.0)
    in_slot = rank[:, None, :] == jnp.arange(capacity, dtype=jnp.float32)[None, :, None]
    slot_weight = jnp.sum(jnp.where(in_slot, token_weight.T[:, None, :], 0.0), axis=2)
    pick = in_slot.astype(jnp.bfloat16).reshape(experts * capacity, tokens_here)
    send_input = jnp.dot(pick, own_stream, preferred_element_type=jnp.float32).astype(jnp.bfloat16)
    send_grad = (
        slot_weight.reshape(-1, 1)
        * jnp.dot(pick, own_cotangent, preferred_element_type=jnp.float32)
    ).astype(jnp.bfloat16)
    got_input = to_owners(send_input, sp_devices)
    rows_input = lax.all_gather(got_input, "tp", axis=1, tiled=True)
    send_grad, got_input = lax.optimization_barrier((send_grad, got_input))
    got_grad = to_owners(send_grad, sp_devices)
    rows_grad = lax.all_gather(got_grad, "tp", axis=1, tiled=True)
    mixed = inner_gate.astype(jnp.float32) * conv_input.astype(jnp.float32)
    previous = passed_along(mixed[tokens_here - 2 :], "sp", 1)
    extended = jnp.concatenate([previous, mixed], axis=0)
    conv_out = (
        conv_taps[0] * extended[:tokens_here]
        + conv_taps[1] * extended[1 : tokens_here + 1]
        + conv_taps[2] * extended[2:]
    )
    mixer_out = (outer_gate.astype(jnp.float32) * conv_out).astype(jnp.bfloat16)
    conv_out, mixer_out, rows_grad = lax.optimization_barrier((conv_out, mixer_out, rows_grad))
    w_gate = gate_proj[0]
    w_up = up_proj[0]
    w_down = down_proj[0]
    gate = jnp.dot(rows_input, w_gate, preferred_element_type=jnp.float32)
    up = jnp.dot(rows_input, w_up, preferred_element_type=jnp.float32)
    sig = jax.nn.sigmoid(gate)
    silu_gate = gate * sig
    hidden = (silu_gate * up).astype(jnp.bfloat16)
    across = (((1,), (1,)), ((), ()))
    d_hidden = lax.dot_general(rows_grad, w_down, across, preferred_element_type=jnp.float32)
    d_gate = (d_hidden * up * sig * (1.0 + gate * (1.0 - sig))).astype(jnp.bfloat16)
    d_up = (d_hidden * silu_gate).astype(jnp.bfloat16)
    grad_down = lax.dot_general(
        hidden, rows_grad, over_rows, preferred_element_type=jnp.float32
    ).astype(jnp.bfloat16)
    grad_gate = lax.dot_general(
        rows_input, d_gate, over_rows, preferred_element_type=jnp.float32
    ).astype(jnp.bfloat16)
    grad_up = lax.dot_general(
        rows_input, d_up, over_rows, preferred_element_type=jnp.float32
    ).astype(jnp.bfloat16)
    chunks = 2
    piece = capacity // chunks
    shape = (sp_devices, chunks, piece, d_gate.shape[1])
    gate_pieces = d_gate.reshape(shape)
    up_pieces = d_up.reshape(shape)
    shares = []
    for c in range(chunks):
        shares.append(
            reduced_quarter(
                gate_pieces[:, c].reshape(-1, shape[3]),
                up_pieces[:, c].reshape(-1, shape[3]),
                w_gate,
                w_up,
            )
        )
    shares[0], grad_down, grad_gate, grad_up = lax.optimization_barrier(
        (shares[0], grad_down, grad_gate, grad_up)
    )
    moe_grad = own_cotangent.astype(jnp.float32)
    pick_pieces = pick.reshape(experts, chunks, piece, tokens_here)
    for c in range(chunks):
        returned = to_owners(shares[c], sp_devices)
        moe_grad = moe_grad + lax.dot_general(
            pick_pieces[:, c].reshape(-1, tokens_here), returned, over_rows,
            preferred_element_type=jnp.float32,
        )
    stream_part = moe_grad.astype(jnp.bfloat16)
    stream_grad = lax.all_gather(stream_part, "tp", axis=1, tiled=True)
    own_projection = lax.dot_general(
        stream_grad, mixer_out, over_rows, preferred_element_type=jnp.float32
    ).astype(jnp.bfloat16)
    projections = to_owners(own_projection, sp_devices)
    grad_projection = jnp.sum(
        projections.astype(jnp.float32).reshape(sp_devices, -1, projections.shape[1]), axis=0
    )
    d_mixer = jnp.dot(stream_grad, out_proj, preferred_element_type=jnp.float32)
    grad_outer = d_mixer * conv_out
    d_conv = d_mixer * outer_gate.astype(jnp.float32)
    following = passed_along(d_conv[:2], "sp", -1)
    trailing = jnp.concatenate([d_conv, following], axis=0)
    d_mixed = (
        conv_taps[2] * trailing[:tokens_here]
        + conv_taps[1] * trailing[1 : tokens_here + 1]
        + conv_taps[0] * trailing[2:]
    )
    grad_inner = d_mixed * conv_input.astype(jnp.float32)
    grad_input = d_mixed * inner_gate.astype(jnp.float32)
    return (
        grad_gate[None],
        grad_up[None],
        grad_down[None],
        grad_projection,
        grad_outer,
        grad_inner,
        grad_input,
    )


def solution(mesh):
    placed = (
        P("sp", None),
        P("sp", None),
        P("sp", None),
        P("sp", None),
        P("sp", None, "tp"),
        P("sp", None, "tp"),
        P("sp", "tp", None),
        P("sp", "tp"),
        P("sp", "tp"),
        P("sp", "tp"),
        P(None, "tp"),
        P(None, "tp"),
    )
    return jax.shard_map(
        shards,
        mesh=mesh,
        in_specs=placed,
        out_specs=(
            P("sp", None, "tp"),
            P("sp", None, "tp"),
            P("sp", "tp", None),
            P("sp", "tp"),
            P("sp", "tp"),
            P("sp", "tp"),
            P("sp", "tp"),
        ),
        check_vma=False,
    )
```

profile of v0, /device:TPU:7, one launch (start us, length us, event | category | flops | bytes accessed | tf_op | source)
XLA Modules:
  0.0 226.3 jit_solution(2613695500812486552)
XLA Ops:
  7.2 0.0 copy-start
  7.2 0.0 all-gather.6.cloned.1.call-start
  7.3 0.8 fusion.26
  8.0 0.1 convolution_select_fusion
  8.2 0.2 bitcast_compare_fusion
  8.4 0.0 copy-done
  8.4 0.5 convolution_convert_fusion.4
  8.9 30.3 %all_to_all.25 = bf16[8,128,512]{2,1,0:T(8,128)(2,1)} all-to-all(bf16[8,128,512]{2,1,0:T(8,128)(2,1)S(1)} %bitcast.91), channel_id=1, replica_groups=mesh['sp'=8,'tp'=4] {'sp'}, dimensions={0} | all-to-all | bytes 2097152 | tf_op jit(solution)/shard_map/all_to_all | solution.py:15
  39.2 0.0 all-gather.6.cloned.1.call-update
  39.2 0.0 all-gather.4.cloned.1.call-start
  39.3 0.2 select_reduce_fusion
  39.5 0.0 copy-start.5
  39.6 1.4 multiply_convert_fusion
  41.0 28.8 %all_to_all.26 = bf16[8,128,512]{2,1,0:T(8,128)(2,1)} all-to-all(bf16[8,128,512]{2,1,0:T(8,128)(2,1)S(1)} %bitcast.90), channel_id=1, replica_groups=mesh['sp'=8,'tp'=4] {'sp'}, dimensions={0} | all-to-all | bytes 2097152 | tf_op jit(solution)/shard_map/all_to_all | solution.py:15
  69.8 0.0 all-gather.4.cloned.1.call-update
  69.9 2.4 %collective-permute-start = (f32[2,128]{1,0:T(2,128)S(1)}, f32[2,128]{1,0:T(2,128)S(1)}, u32[]{:S(2)}, u32[]{:S(2)}) collective-permute-start(f32[2,128]{1,0:T(2,128)S(1)} %slice.95), channel_id=1, source_target_pairs={{0,4},{4,8},{8,12},{12,16},{16,20},{20,24},{24,28},{1,5},{5,9},{9,... | collective-permute-start | bytes 3080 | tf_op jit(solution)/shard_map/ppermute | solution.py:10
  72.3 1.7 dynamic-slice_bitcast_fusion.5
  74.0 0.2 collective-permute-done
  74.2 0.6 copy-done.14
  74.7 1.4 fusion.23
  76.2 4.9 %fusion.1 = f32[1024,256]{1,0:T(8,128)} fusion(bf16[1024,2048]{1,0:T(8,128)(2,1)} %all-gather.6.cloned.1.call-done, bf16[1,2048,256]{2,1,0:T(8,128)(2,1)} %param.16), kind=kOutput, calls=%fused_computation.14 | convolution fusion | flops 1073741824 | bytes 6291456 | tf_op jit(solution)/shard_map/dot_general | solution.py:111
  81.1 2.2 fusion.3
  83.3 26.2 %all-gather.4.cloned.1.call-done = bf16[1024,2048]{1,0:T(8,128)(2,1)} async-done(((bf16[1024,512]{1,0:T(8,128)(2,1)}), bf16[1024,2048]{1,0:T(8,128)(2,1)}) %all-gather.4.cloned.1.call-update) | async-done | bytes 4194320 | tf_op jit(solution)/shard_map/all_gather | solution.py:97
  109.5 4.6 %multiply_convert_fusion.2 = (bf16[1024,256]{1,0:T(8,128)(2,1)S(1)}, bf16[1024,256]{1,0:T(8,128)(2,1)S(1)}) fusion(f32[1024,256]{1,0:T(8,128)} %fusion.1, f32[1024,256]{1,0:T(8,128)} %fusion.3, bf16[1024,2048]{1,0:T(8,128)(2,1)} %all-gather.4.cloned.1.call-done, bf16[1,256,2048]{2,1,0:T(8,128)(2,1)} %param.18), kind=kOutput, calls=%fused_computation.27 | convolution fusion | flops 1077149696 | bytes 8388608 | tf_op jit(solution)/shard_map/dot_general | solution.py:117
  114.1 0.5 fusion.8
  114.6 0.5 fusion.9
  115.1 0.5 fusion.11
  115.6 0.5 fusion.10
  116.1 1.5 add_convert_fusion
  117.5 0.3 collective-permute-start.3
  117.8 0.5 add_convert_fusion.2
  118.3 0.3 collective-permute-start.1
  118.6 0.5 add_convert_fusion.3
  119.1 0.5 add_convert_fusion.1
  119.6 1.2 copy-done.16
  120.8 2.3 %convolution_convert_fusion = bf16[2048,256]{1,0:T(8,128)(2,1)} fusion(bf16[1024,2048]{1,0:T(8,128)(2,1)S(1)} %copy-done.16, bf16[1024,256]{1,0:T(8,128)(2,1)S(1)} %get-tuple-element.27), kind=kOutput, calls=%fused_computation | convolution fusion | flops 1074266112 | bytes 5767168 | tf_op jit(solution)/shard_map/dot_general | solution.py:126
  123.2 2.3 %convolution_convert_fusion.1 = bf16[2048,256]{1,0:T(8,128)(2,1)} fusion(bf16[1024,2048]{1,0:T(8,128)(2,1)S(1)} %copy-done.16, bf16[1024,256]{1,0:T(8,128)(2,1)S(1)} %get-tuple-element.28), kind=kOutput, calls=%fused_computation.1 | convolution fusion | flops 1074266112 | bytes 5767168 | tf_op jit(solution)/shard_map/dot_general | solution.py:123
  125.5 0.2 add_convert_fusion.7
  125.7 1.3 collective-permute-start.2
  127.0 2.3 %convolution_convert_fusion.2 = bf16[256,2048]{1,0:T(8,128)(2,1)} fusion(bf16[1024,2048]{1,0:T(8,128)(2,1)S(1)} %copy-done.17, f32[1024,256]{1,0:T(8,128)S(1)} %copy-done.19, f32[1024,256]{1,0:T(8,128)S(1)} %copy-done.18), kind=kOutput, calls=%fused_computation.2 | convolution fusion | flops 1075838976 | bytes 7340032 | tf_op jit(solution)/shard_map/dot_general | solution.py:120
  129.3 9.7 %collective-permute-done.2 = bf16[512,512]{1,0:T(8,128)(2,1)S(1)} collective-permute-done((bf16[512,512]{1,0:T(8,128)(2,1)S(1)}, bf16[512,512]{1,0:T(8,128)(2,1)S(1)}, u32[]{:S(2)}, u32[]{:S(2)}) %collective-permute-start.2) | collective-permute-done | bytes 524320 | tf_op jit(solution)/shard_map/ppermute | solution.py:41
  139.0 1.1 add_convert_fusion.6
  140.1 5.5 %all-to-all-start.2 = ((bf16[8,64,512]{2,1,0:T(8,128)(2,1)}), bf16[8,64,512]{2,1,0:T(8,128)(2,1)S(1)}, u32[]{:S(2)}, u32[]{:S(2)}) async-start(bf16[8,64,512]{2,1,0:T(8,128)(2,1)} %bitcast.31), calls=%async_computation.2 | async-start | bytes 1048576 | tf_op jit(solution)/shard_map/all_to_all | solution.py:15
  145.6 1.2 add_convert_fusion.5
  146.8 1.3 collective-permute-start.4
  148.0 10.6 %collective-permute-done.4 = bf16[512,512]{1,0:T(8,128)(2,1)S(1)} collective-permute-done((bf16[512,512]{1,0:T(8,128)(2,1)S(1)}, bf16[512,512]{1,0:T(8,128)(2,1)S(1)}, u32[]{:S(2)}, u32[]{:S(2)}) %collective-permute-start.4) | collective-permute-done | bytes 524320 | tf_op jit(solution)/shard_map/ppermute | solution.py:41
  158.7 2.1 add_convert_fusion.4
  160.7 5.4 %all-to-all-start.3 = ((bf16[8,64,512]{2,1,0:T(8,128)(2,1)}), bf16[8,64,512]{2,1,0:T(8,128)(2,1)S(1)}, u32[]{:S(2)}, u32[]{:S(2)}) async-start(bf16[8,64,512]{2,1,0:T(8,128)(2,1)} %bitcast.36), calls=%async_computation.3 | async-start | bytes 1048576 | tf_op jit(solution)/shard_map/all_to_all | solution.py:15
  166.2 0.2 broadcast_compare_fusion
  166.4 0.2 fusion.42
  166.6 1.3 convolution_add_fusion.1
  167.9 9.5 %all-to-all-done.3 = bf16[8,64,512]{2,1,0:T(8,128)(2,1)S(1)} async-done(((bf16[8,64,512]{2,1,0:T(8,128)(2,1)}), bf16[8,64,512]{2,1,0:T(8,128)(2,1)S(1)}, u32[]{:S(2)}, u32[]{:S(2)}) %all-to-all-start.3) | async-done | bytes 524320 | tf_op jit(solution)/shard_map/all_to_all | solution.py:15
  177.4 1.0 fusion
  178.4 0.0 all-gather.8.cloned.1.call-update
  178.5 18.7 %all-gather.8.cloned.1.call-done = bf16[256,2048]{1,0:T(8,128)(2,1)} async-done(((bf16[256,512]{1,0:T(8,128)(2,1)}), bf16[256,2048]{1,0:T(8,128)(2,1)}) %all-gather.8.cloned.1.call-update) | async-done | bytes 1048592 | tf_op jit(solution)/shard_map/all_gather | solution.py:156
  197.2 2.6 %convolution_convert_fusion.3 = bf16[2048,128]{1,0:T(8,128)(2,1)} fusion(bf16[256,2048]{1,0:T(8,128)(2,1)} %all-gather.8.cloned.1.call-done, bf16[256,128]{1,0:T(8,128)(2,1)S(1)} %copy-done.6), kind=kOutput, calls=%fused_computation.3 | convolution fusion | flops 134479872 | bytes 1638400 | tf_op jit(solution)/shard_map/dot_general | solution.py:157
  199.8 5.5 %all-to-all-start.4 = ((bf16[8,256,128]{2,1,0:T(8,128)(2,1)}), bf16[8,256,128]{2,1,0:T(8,128)(2,1)S(1)}, u32[]{:S(2)}, u32[]{:S(2)}) async-start(bf16[8,256,128]{2,1,0:T(8,128)(2,1)} %bitcast.38), calls=%async_computation.4 | async-start | bytes 1048576 | tf_op jit(solution)/shard_map/all_to_all | solution.py:15
  205.3 1.1 convert_multiply_fusion
  206.4 1.9 collective-permute-start.5
  208.3 3.3 %collective-permute-done.5 = f32[2,128]{1,0:T(2,128)S(1)} collective-permute-done((f32[2,128]{1,0:T(2,128)S(1)}, f32[2,128]{1,0:T(2,128)S(1)}, u32[]{:S(2)}, u32[]{:S(2)}) %collective-permute-start.5) | collective-permute-done | bytes 1056 | tf_op jit(solution)/shard_map/ppermute | solution.py:10
  211.6 0.7 convert_multiply_fusion.4
  212.3 0.7 convert_multiply_fusion.2
  213.0 6.1 %all-to-all-done.4 = bf16[8,256,128]{2,1,0:T(8,128)(2,1)S(1)} async-done(((bf16[8,256,128]{2,1,0:T(8,128)(2,1)}), bf16[8,256,128]{2,1,0:T(8,128)(2,1)S(1)}, u32[]{:S(2)}, u32[]{:S(2)}) %all-to-all-start.4) | async-done | bytes 524320 | tf_op jit(solution)/shard_map/all_to_all | solution.py:15
  219.0 0.7 convert_reduce_fusion
  (49 shorter events, 0.2 us)
Async XLA Ops:
  7.2 1.2 copy-start
  7.2 69.0 %all-gather.6.cloned.1.call-start = ((), (), s32[]{:S(2)}) async-start(), calls=%async_computation.6 | async-start | bytes 5242880 | tf_op jit(solution)/shard_map/all_gather | solution.py:94
  8.4 30.9 %copy-start.9 = (s32[256,2]{0,1:T(2,128)S(1)}, s32[256,2]{0,1:T(2,128)}, u32[]{:S(2)}) copy-start(s32[256,2]{0,1:T(2,128)} %param.14) | copy-start | bytes 6148
  8.4 30.9 %copy-start.12 = (f32[256,2]{0,1:T(2,128)S(1)}, f32[256,2]{0,1:T(2,128)}, u32[]{:S(2)}) copy-start(f32[256,2]{0,1:T(2,128)} %param.15) | copy-start | bytes 6148
  39.2 70.3 %all-gather.4.cloned.1.call-start = ((), (), s32[]{:S(2)}) async-start(), calls=%async_computation.5 | async-start | bytes 5242880 | tf_op jit(solution)/shard_map/all_gather | solution.py:97
  39.5 30.3 %copy-start.5 = (bf16[256,128]{1,0:T(8,128)(2,1)S(1)}, bf16[256,128]{1,0:T(8,128)(2,1)}, u32[]{:S(2)}) copy-start(bf16[256,128]{1,0:T(8,128)(2,1)} %param.21) | copy-start | bytes 196612
  39.5 30.3 %copy-start.7 = (bf16[256,128]{1,0:T(8,128)(2,1)S(1)}, bf16[256,128]{1,0:T(8,128)(2,1)}, u32[]{:S(2)}) copy-start(bf16[256,128]{1,0:T(8,128)(2,1)} %param.20) | copy-start | bytes 196612
  41.0 31.3 %copy-start.13 = (f32[3,128]{1,0:T(4,128)S(1)}, f32[3,128]{1,0:T(4,128)}, u32[]{:S(2)}) copy-start(f32[3,128]{1,0:T(4,128)} %param.22) | copy-start | bytes 4612
  69.9 4.3 %collective-permute-start = (f32[2,128]{1,0:T(2,128)S(1)}, f32[2,128]{1,0:T(2,128)S(1)}, u32[]{:S(2)}, u32[]{:S(2)}) collective-permute-start(f32[2,128]{1,0:T(2,128)S(1)} %slice.95), channel_id=1, source_target_pairs={{0,4},{4,8},{8,12},{12,16},{16,20},{20,24},{24,28},{1,5},{5,9},{9,... | collective-permute-start | bytes 3080 | tf_op jit(solution)/shard_map/ppermute | solution.py:10
  72.3 2.4 %copy-start.10 = (f32[128]{0:T(128)}, f32[128]{0:T(128)S(1)}, u32[]{:S(2)}) copy-start(f32[128]{0:T(128)S(1)} %get-tuple-element.47) | copy-start | bytes 1540
  72.3 2.4 %copy-start.4 = (bf16[256,128]{1,0:T(8,128)(2,1)S(1)}, bf16[256,128]{1,0:T(8,128)(2,1)}, u32[]{:S(2)}) copy-start(bf16[256,128]{1,0:T(8,128)(2,1)} %param.19) | copy-start | bytes 196612
  74.2 0.6 copy-start.14
  76.2 4.9 %copy-start.2 = (bf16[1,2048,256]{2,1,0:T(8,128)(2,1)S(1)}, bf16[1,2048,256]{2,1,0:T(8,128)(2,1)}, u32[]{:S(2)}) copy-start(bf16[1,2048,256]{2,1,0:T(8,128)(2,1)} %param.17) | copy-start | bytes 3145732
  76.2 4.9 %copy-start.15 = (bf16[1024,2048]{1,0:T(8,128)(2,1)S(1)}, bf16[1024,2048]{1,0:T(8,128)(2,1)}, u32[]{:S(2)}) copy-start(bf16[1024,2048]{1,0:T(8,128)(2,1)} %all-gather.6.cloned.1.call-done) | copy-start | bytes 12582916
  117.5 28.0 %collective-permute-start.3 = (bf16[512,1024]{1,0:T(8,128)(2,1)}, bf16[512,1024]{1,0:T(8,128)(2,1)}, u32[]{:S(2)}, u32[]{:S(2)}) collective-permute-start(bf16[512,1024]{1,0:T(8,128)(2,1)} %add_convert_fusion), channel_id=1, source_target_pairs={{0,1},{1,0},{2,3},{3,2},{4,5},{5,4},{6,7},{7,6},{8,9},{9,8},{10,11... | collective-permute-start | bytes 3145736 | tf_op jit(solution)/shard_map/ppermute | solution.py:41
  118.3 7.2 %collective-permute-start.1 = (bf16[512,1024]{1,0:T(8,128)(2,1)S(1)}, bf16[512,1024]{1,0:T(8,128)(2,1)S(1)}, u32[]{:S(2)}, u32[]{:S(2)}) collective-permute-start(bf16[512,1024]{1,0:T(8,128)(2,1)S(1)} %add_convert_fusion.2), channel_id=1, source_target_pairs={{0,1},{1,0},{2,3},{3,2},{4,5},{5,4},{6,7},{7,6},{8,9},{9,8},{10,11... | collective-permute-start | bytes 3145736 | tf_op jit(solution)/shard_map/ppermute | solution.py:41
  118.6 2.2 copy-start.16
  123.2 3.8 %copy-start.17 = (bf16[1024,2048]{1,0:T(8,128)(2,1)S(1)}, bf16[1024,2048]{1,0:T(8,128)(2,1)}, u32[]{:S(2)}) copy-start(bf16[1024,2048]{1,0:T(8,128)(2,1)} %all-gather.4.cloned.1.call-done) | copy-start | bytes 12582916
  123.2 3.8 %copy-start.18 = (f32[1024,256]{1,0:T(8,128)S(1)}, f32[1024,256]{1,0:T(8,128)}, u32[]{:S(2)}) copy-start(f32[1024,256]{1,0:T(8,128)} %fusion.1) | copy-start | bytes 3145732
  123.2 3.8 %copy-start.19 = (f32[1024,256]{1,0:T(8,128)S(1)}, f32[1024,256]{1,0:T(8,128)}, u32[]{:S(2)}) copy-start(f32[1024,256]{1,0:T(8,128)} %fusion.3) | copy-start | bytes 3145732
  125.7 13.3 %collective-permute-start.2 = (bf16[512,512]{1,0:T(8,128)(2,1)S(1)}, bf16[512,512]{1,0:T(8,128)(2,1)S(1)}, u32[]{:S(2)}, u32[]{:S(2)}) collective-permute-start(bf16[512,512]{1,0:T(8,128)(2,1)S(1)} %add_convert_fusion.7), channel_id=1, source_target_pairs={{0,2},{1,3},{2,0},{3,1},{4,6},{5,7},{6,4},{7,5},{8,10},{9,11},{10,... | collective-permute-start | bytes 1572872 | tf_op jit(solution)/shard_map/ppermute | solution.py:41
  140.1 20.7 %all-to-all-start.2 = ((bf16[8,64,512]{2,1,0:T(8,128)(2,1)}), bf16[8,64,512]{2,1,0:T(8,128)(2,1)S(1)}, u32[]{:S(2)}, u32[]{:S(2)}) async-start(bf16[8,64,512]{2,1,0:T(8,128)(2,1)} %bitcast.31), calls=%async_computation.2 | async-start | bytes 1048576 | tf_op jit(solution)/shard_map/all_to_all | solution.py:15
  146.8 11.9 %collective-permute-start.4 = (bf16[512,512]{1,0:T(8,128)(2,1)S(1)}, bf16[512,512]{1,0:T(8,128)(2,1)S(1)}, u32[]{:S(2)}, u32[]{:S(2)}) collective-permute-start(bf16[512,512]{1,0:T(8,128)(2,1)S(1)} %add_convert_fusion.5), channel_id=1, source_target_pairs={{0,2},{1,3},{2,0},{3,1},{4,6},{5,7},{6,4},{7,5},{8,10},{9,11},{10,... | collective-permute-start | bytes 1572872 | tf_op jit(solution)/shard_map/ppermute | solution.py:41
  160.7 16.6 %all-to-all-start.3 = ((bf16[8,64,512]{2,1,0:T(8,128)(2,1)}), bf16[8,64,512]{2,1,0:T(8,128)(2,1)S(1)}, u32[]{:S(2)}, u32[]{:S(2)}) async-start(bf16[8,64,512]{2,1,0:T(8,128)(2,1)} %bitcast.36), calls=%async_computation.3 | async-start | bytes 1048576 | tf_op jit(solution)/shard_map/all_to_all | solution.py:15
  166.2 31.0 %copy-start.6 = (bf16[256,128]{1,0:T(8,128)(2,1)S(1)}, bf16[256,128]{1,0:T(8,128)(2,1)}, u32[]{:S(2)}) copy-start(bf16[256,128]{1,0:T(8,128)(2,1)} %get-tuple-element.21) | copy-start | bytes 196612
  166.2 31.0 %all-gather.8.cloned.1.call-start = ((), (), s32[]{:S(2)}) async-start(), calls=%async_computation.7 | async-start | bytes 1310720 | tf_op jit(solution)/shard_map/all_gather | solution.py:156
  177.4 27.9 %copy-start.3 = (bf16[2048,128]{1,0:T(8,128)(2,1)S(1)}, bf16[2048,128]{1,0:T(8,128)(2,1)}, u32[]{:S(2)}) copy-start(bf16[2048,128]{1,0:T(8,128)(2,1)} %param.23) | copy-start | bytes 1572868
  178.4 33.1 %copy-start.8 = (bf16[256,128]{1,0:T(8,128)(2,1)S(1)}, bf16[256,128]{1,0:T(8,128)(2,1)}, u32[]{:S(2)}) copy-start(bf16[256,128]{1,0:T(8,128)(2,1)} %param.20) | copy-start | bytes 196612
  178.5 33.1 %copy-start.11 = (f32[128]{0:T(128)S(1)}, f32[128]{0:T(128)}, u32[]{:S(2)}) copy-start(f32[128]{0:T(128)} %copy-done.10) | copy-start | bytes 1540
  197.2 8.1 %copy-start.1 = (bf16[256,2048]{1,0:T(8,128)(2,1)S(1)}, bf16[256,2048]{1,0:T(8,128)(2,1)}, u32[]{:S(2)}) copy-start(bf16[256,2048]{1,0:T(8,128)(2,1)} %all-gather.8.cloned.1.call-done) | copy-start | bytes 3145732
  199.8 19.3 %all-to-all-start.4 = ((bf16[8,256,128]{2,1,0:T(8,128)(2,1)}), bf16[8,256,128]{2,1,0:T(8,128)(2,1)S(1)}, u32[]{:S(2)}, u32[]{:S(2)}) async-start(bf16[8,256,128]{2,1,0:T(8,128)(2,1)} %bitcast.38), calls=%async_computation.4 | async-start | bytes 1048576 | tf_op jit(solution)/shard_map/all_to_all | solution.py:15
  206.4 5.2 %collective-permute-start.5 = (f32[2,128]{1,0:T(2,128)S(1)}, f32[2,128]{1,0:T(2,128)S(1)}, u32[]{:S(2)}, u32[]{:S(2)}) collective-permute-start(f32[2,128]{1,0:T(2,128)S(1)} %slice.112), channel_id=1, source_target_pairs={{4,0},{8,4},{12,8},{16,12},{20,16},{24,20},{28,24},{5,1},{9,5},{13... | collective-permute-start | bytes 3080 | tf_op jit(solution)/shard_map/ppermute | solution.py:10
Sparse Core Ops, SparseCore 0:
  39.4 34.0 all-gather.5
  75.0 34.4 all-gather.3
  178.6 18.5 all-gather.7
where the time goes:
time: 230 us; the launch traced here: 226 us
  waiting for transfers between devices  84.3 us (37%)
  blocking collectives  59.1 us (26%)
  matrix products  31.5 us (14%)
  starting transfers between devices  23.9 us (10%)
  between operations  14.1 us (6%)
  other arithmetic  9.56 us (4%)
  local copies, waits for them, and re-layouts  3.85 us (2%)
    all_to_all x2, blocking collectives, to_owners(): lax.all_to_all(blocks, 'sp', split_axis=0, concat_axis=0, tiled=True)  59.1 us
    all_gather x1, waiting for transfers between devices, shards(): rows_grad = lax.all_gather(got_grad, 'tp', axis=1, tiled=True)  26.2 us
    ppermute x4, waiting for transfers between devices, swapped(): return lax.ppermute(x, 'tp', [(i, i ^ flip) for i in range(devices)])  20.3 us
    all_gather x1, waiting for transfers between devices, shards(): stream_grad = lax.all_gather(stream_part, 'tp', axis=1, tiled=True)  18.7 us
    all_to_all x3, starting transfers between devices, to_owners(): lax.all_to_all(blocks, 'sp', split_axis=0, concat_axis=0, tiled=True)  16.5 us
    all_to_all x3, waiting for transfers between devices, to_owners(): lax.all_to_all(blocks, 'sp', split_axis=0, concat_axis=0, tiled=True)  15.5 us
    dot_general x1, matrix products, shards(): gate = jnp.dot(rows_input, w_gate, preferred_element_type=jnp.float32)  4.86 us
  transfers between devices with their start and end apart: 12, of which 8 were waited for; matrix products, arithmetic and copies ran while one was open for 13% of the time, Pallas kernels for 0%

commit v1 on v0

--- a/solution.py
+++ b/solution.py
@@ -1,6 +1,10 @@
+import functools
+
 import jax
 import jax.numpy as jnp
 from jax import lax
+from jax.experimental import pallas as pl
+from jax.experimental.pallas import tpu as pltpu
 from jax.sharding import PartitionSpec as P
 
 
@@ -184,6 +188,538 @@
     )
 
 
+MESH = pl.DeviceIdType.MESH
+
+
+def flipped(index, flips):
+    place = 1
+    while place <= flips:
+        if (flips // place) % 2:
+            index = index + place * (1 - 2 * ((index // place) % 2))
+        place *= 2
+    return index
+
+
+def fused(
+    sp_devices,
+    groups,
+    cot_ref,
+    stream_ref,
+    pick_ref,
+    slot_weight_ref,
+    outer_ref,
+    inner_ref,
+    input_ref,
+    taps_ref,
+    out_proj_ref,
+    w_gate_ref,
+    w_up_ref,
+    w_down_ref,
+    grad_gate_ref,
+    grad_up_ref,
+    grad_down_ref,
+    grad_proj_ref,
+    grad_outer_ref,
+    grad_inner_ref,
+    grad_input_ref,
+    rows,
+    a_send,
+    w_pair,
+    w_down,
+    hidden,
+    d_pair,
+    kept,
+    near_got,
+    core_send,
+    core_got,
+    y_send,
+    y_got,
+    back_send,
+    back_got,
+    stream_grad,
+    proj_send,
+    proj_got,
+    before,
+    after,
+    conv_out,
+    mixer_out,
+    load_sem,
+    a_sem,
+    b_sem,
+    c_sem,
+    core_sem,
+    y_sem,
+    back_sem,
+    gather_sem,
+    proj_sem,
+    conv_sem,
+):
+    f32, bf16 = jnp.float32, jnp.bfloat16
+    me = lax.axis_index("sp")
+    t = lax.axis_index("tp")
+    t_core, t_y, t_far = flipped(t, 1), flipped(t, 2), flipped(t, 3)
+    tokens, width = stream_ref.shape
+    capacity = pick_ref.shape[0] // sp_devices
+    units = hidden.shape[1]
+    quarter = width // lax.axis_size("tp")
+    per = width // sp_devices
+    over_rows = (((0,), (0,)), ((), ()))
+    across = (((1,), (1,)), ((), ()))
+
+    def columns(q):
+        return pl.ds(pl.multiple_of(q * quarter, quarter), quarter)
+
+    def block(k):
+        return pl.ds(k * capacity, capacity)
+
+    def remote(src, dst, sems, sp, tp):
+        return pltpu.make_async_remote_copy(
+            src_ref=src,
+            dst_ref=dst,
+            send_sem=sems[0],
+            recv_sem=sems[1],
+            device_id=(sp, tp),
+            device_id_type=MESH,
+        )
+
+    peers = [(flipped(me, k), t) for k in range(1, sp_devices)] + [(me, t_core), (me, t_y)]
+    barrier = pltpu.get_barrier_semaphore()
+    for peer in peers:
+        pl.semaphore_signal(barrier, inc=1, device_id=peer, device_id_type=MESH)
+
+    loads = [
+        pltpu.make_async_copy(w_gate_ref, w_pair.at[:, pl.ds(0, units)], load_sem.at[0]),
+        pltpu.make_async_copy(w_up_ref, w_pair.at[:, pl.ds(units, units)], load_sem.at[1]),
+        pltpu.make_async_copy(w_down_ref, w_down, load_sem.at[2]),
+    ]
+    for load in loads:
+        load.start()
+    mixed = inner_ref[...].astype(f32) * input_ref[...].astype(f32)
+    before[pl.ds(8, tokens), :] = mixed
+
+    pl.semaphore_wait(barrier, len(peers))
+
+    others = range(1, sp_devices)
+    a, b, c_near, c_far, back = {}, {}, {}, {}, {}
+    for k in others:
+        mine, theirs = rows.at[:, block(k), columns(t)], rows.at[:, block(k), columns(t_y)]
+        peer = flipped(me, k)
+        a[k] = remote(a_send.at[k - 1], mine, (a_sem.at[0, k], a_sem.at[1, k]), peer, t)
+        b[k] = remote(mine, mine, (b_sem.at[0, k], b_sem.at[1, k]), me, t_y)
+        c_near[k] = remote(mine, mine, (c_sem.at[0, k], c_sem.at[1, k]), me, t_core)
+        c_far[k] = remote(theirs, theirs, (c_sem.at[2, k], c_sem.at[3, k]), me, t_core)
+        back[k] = remote(
+            back_send.at[block(k)],
+            back_got.at[pl.ds(pl.multiple_of(me * capacity, capacity), capacity)],
+            (back_sem.at[0, k], back_sem.at[1, k]),
+            peer,
+            t,
+        )
+
+    def slots_of(k):
+        return pl.ds(pl.multiple_of(flipped(me, k) * capacity, capacity), capacity)
+
+    for k in others:
+        pick = pick_ref[slots_of(k), :]
+        a_send[k - 1, 0] = jnp.dot(
+            pick, stream_ref[:, columns(t)], preferred_element_type=f32
+        ).astype(bf16)
+        a_send[k - 1, 1] = (
+            slot_weight_ref[slots_of(k), :]
+            * jnp.dot(pick, cot_ref[:, columns(t)], preferred_element_type=f32)
+        ).astype(bf16)
+        a[k].start()
+
+    to_next = remote(
+        before.at[pl.ds(tokens, 8)],
+        before.at[pl.ds(0, 8)],
+        (conv_sem.at[0], conv_sem.at[1]),
+        me + 1,
+        t,
+    )
+    to_previous = remote(
+        after.at[pl.ds(0, 8)],
+        after.at[pl.ds(tokens, 8)],
+        (conv_sem.at[2], conv_sem.at[3]),
+        me - 1,
+        t,
+    )
+
+    @pl.when(me < sp_devices - 1)
+    def _():
+        to_next.start()
+
+    pick = pick_ref[slots_of(0), :]
+    rows[0, block(0), :] = jnp.dot(pick, stream_ref[...], preferred_element_type=f32).astype(bf16)
+    rows[1, block(0), :] = (
+        slot_weight_ref[slots_of(0), :]
+        * jnp.dot(pick, cot_ref[...], preferred_element_type=f32)
+    ).astype(bf16)
+
+    @pl.when(me == 0)
+    def _():
+        before[pl.ds(0, 8), :] = jnp.zeros((8, before.shape[1]), f32)
+
+    @pl.when(me > 0)
+    def _():
+        to_next.wait_recv()
+
+    conv = (
+        taps_ref[0:1, :] * before[pl.ds(6, tokens), :]
+        + taps_ref[1:2, :] * before[pl.ds(7, tokens), :]
+        + taps_ref[2:3, :] * before[pl.ds(8, tokens), :]
+    )
+    conv_out[...] = conv
+    mixer_out[...] = (outer_ref[...].astype(f32) * conv).astype(bf16)
+    for load in loads:
+        load.wait()
+
+    core, y_hop = {}, {}
+    for g, ks in enumerate(groups):
+        span = pl.ds(ks[0] * capacity, len(ks) * capacity)
+        core[g] = [
+            remote(
+                core_send.at[i, span], core_got.at[i, span],
+                (core_sem.at[0, i, g], core_sem.at[1, i, g]), me, t_core,
+            )
+            for i in range(2)
+        ]
+        y_hop[g] = remote(y_send.at[span], y_got.at[span], (y_sem.at[0, g], y_sem.at[1, g]), me, t_y)
+
+    def stage_a(ks):
+        for k in ks:
+            if k:
+                a[k].wait_recv()
+                b[k].start()
+                c_near[k].start()
+
+    def stage_b(ks):
+        for k in ks:
+            if k:
+                b[k].wait_recv()
+                c_far[k].start()
+
+    def stage_c(ks):
+        for k in ks:
+            if k:
+                c_near[k].wait_recv()
+                c_far[k].wait_recv()
+
+    def expert(g, ks):
+        span = pl.ds(ks[0] * capacity, len(ks) * capacity)
+        both = jnp.dot(rows[0, span, :], w_pair[...], preferred_element_type=f32)
+        gate, up = both[:, :units], both[:, units:]
+        d_hidden = lax.dot_general(
+            rows[1, span, :], w_down[...], across, preferred_element_type=f32
+        )
+        sig = jax.nn.sigmoid(gate)
+        silu_gate = gate * sig
+        hidden[span, :] = (silu_gate * up).astype(bf16)
+        d_gate = (d_hidden * up * sig * (1.0 + gate * (1.0 - sig))).astype(bf16)
+        d_up = (d_hidden * silu_gate).astype(bf16)
+        d_pair[span, pl.ds(0, units)] = d_gate
+        d_pair[span, pl.ds(units, units)] = d_up
+
+        def partial(q):
+            return lax.dot_general(
+                d_pair[span, :], w_pair[columns(q), :], across, preferred_element_type=f32
+            ).astype(bf16)
+
+        core_send[1, span, :] = partial(t_far)
+        core_send[0, span, :] = partial(t_core)
+        core[g][1].start()
+        kept[1, span, :] = partial(t_y)
+        core[g][0].start()
+        kept[0, span, :] = partial(t)
+
+    def reduce_core(g, ks):
+        span = pl.ds(ks[0] * capacity, len(ks) * capacity)
+        core[g][1].wait_recv()
+        y_send[span, :] = (
+            kept[1, span, :].astype(f32) + core_got[1, span, :].astype(f32)
+        ).astype(bf16)
+        core[g][0].wait_recv()
+        near_got[span, :] = kept[0, span, :].astype(f32) + core_got[0, span, :].astype(f32)
+        y_hop[g].start()
+
+    def reduce_y(g, ks):
+        span = pl.ds(ks[0] * capacity, len(ks) * capacity)
+        y_hop[g].wait_recv()
+        back_send[span, :] = (near_got[span, :] + y_got[span, :].astype(f32)).astype(bf16)
+        for k in ks:
+            if k:
+                back[k].start()
+            else:
+                own = pl.ds(pl.multiple_of(me * capacity, capacity), capacity)
+                back_got[own, :] = back_send[block(0), :]
+
+    stage_a(groups[0])
+    last = len(groups) - 1
+    for g, ks in enumerate(groups):
+        if g < last:
+            stage_a(groups[g + 1])
+        stage_b(ks)
+        if g:
+            reduce_y(g - 1, groups[g - 1])
+        stage_c(ks)
+        expert(g, ks)
+        if g < last:
+            reduce_core(g, ks)
+
+    step = 2 * units
+
+    def down(j, carry):
+        at = pl.ds(pl.multiple_of(j * step, step), step)
+        grad_down_ref[:, at] = lax.dot_general(
+            hidden[...], rows[1, :, at], over_rows, preferred_element_type=f32
+        ).astype(bf16)
+        return carry
+
+    def gate_up(j, carry):
+        at = pl.ds(pl.multiple_of(j * units, units), units)
+        both = lax.dot_general(
+            rows[0, :, at], d_pair[...], over_rows, preferred_element_type=f32
+        ).astype(bf16)
+        grad_gate_ref[at, :] = both[:, :units]
+        grad_up_ref[at, :] = both[:, units:]
+        return carry
+
+    lax.fori_loop(0, width // step, down, 0)
+    reduce_core(last, groups[last])
+    lax.fori_loop(0, width // units // 2, gate_up, 0)
+    reduce_y(last, groups[last])
+    lax.fori_loop(width // units // 2, width // units, gate_up, 0)
+
+    for k in others:
+        back[k].wait_recv()
+    moe_grad = lax.dot_general(pick_ref[...], back_got[...], over_rows, preferred_element_type=f32)
+    stream_grad[:, columns(t)] = (cot_ref[:, columns(t)].astype(f32) + moe_grad).astype(bf16)
+    part, part_y = stream_grad.at[:, columns(t)], stream_grad.at[:, columns(t_y)]
+    gathers = [
+        remote(part, part, (gather_sem.at[0, 0], gather_sem.at[1, 0]), me, t_y),
+        remote(part, part, (gather_sem.at[0, 1], gather_sem.at[1, 1]), me, t_core),
+        remote(part_y, part_y, (gather_sem.at[0, 2], gather_sem.at[1, 2]), me, t_core),
+    ]
+    gathers[0].start()
+    gathers[1].start()
+    share = quarter // per
+    sends = []
+
+    def project(j, q):
+        piece = stream_grad[:, columns(q)]
+        proj_send[j] = lax.dot_general(
+            piece, mixer_out[...], over_rows, preferred_element_type=f32
+        ).astype(bf16)
+        for i in range(share):
+            owner = q * share + i
+            send = remote(
+                proj_send.at[j, pl.ds(i * per, per)],
+                proj_got.at[me],
+                (proj_sem.at[0, j * share + i], proj_sem.at[1, me]),
+                owner,
+                t,
+            )
+
+            @pl.when(owner != me)
+            def _():
+                send.start()
+
+            @pl.when(owner == me)
+            def _():
+                proj_got[me] = proj_send[j, pl.ds(i * per, per), :]
+
+            sends.append((owner, send))
+        return jnp.dot(piece, out_proj_ref[columns(q), :], preferred_element_type=f32)
+
+    d_mixer = project(0, t)
+    gathers[1].wait_recv()
+    d_mixer = d_mixer + project(1, t_core)
+    gathers[0].wait_recv()
+    gathers[2].start()
+    d_mixer = d_mixer + project(2, t_y)
+    gathers[2].wait_recv()
+    d_mixer = d_mixer + project(3, t_far)
+
+    d_conv = d_mixer * outer_ref[...].astype(f32)
+    after[pl.ds(0, tokens), :] = d_conv
+    grad_outer_ref[...] = d_mixer * conv_out[...]
+
+    @pl.when(me > 0)
+    def _():
+        to_previous.start()
+
+    @pl.when(me == sp_devices - 1)
+    def _():
+        after[pl.ds(tokens, 8), :] = jnp.zeros((8, after.shape[1]), f32)
+
+    @pl.when(me < sp_devices - 1)
+    def _():
+        to_previous.wait_recv()
+
+    d_mixed = (
+        taps_ref[2:3, :] * after[pl.ds(0, tokens), :]
+        + taps_ref[1:2, :] * after[pl.ds(1, tokens), :]
+        + taps_ref[0:1, :] * after[pl.ds(2, tokens), :]
+    )
+    grad_inner_ref[...] = d_mixed * input_ref[...].astype(f32)
+    grad_input_ref[...] = d_mixed * inner_ref[...].astype(f32)
+
+    for k in others:
+        source = flipped(me, k)
+        remote(
+            proj_send.at[0, pl.ds(0, per)],
+            proj_got.at[source],
+            (proj_sem.at[0, 0], proj_sem.at[1, source]),
+            source,
+            t,
+        ).wait_recv()
+    total = proj_got[0].astype(f32)
+    for s in range(1, sp_devices):
+        total = total + proj_got[s].astype(f32)
+    grad_proj_ref[...] = total
+
+    for k in others:
+        for copy in (a[k], b[k], c_near[k], c_far[k], back[k]):
+            copy.wait_send()
+    for g in range(len(groups)):
+        core[g][0].wait_send()
+        core[g][1].wait_send()
+        y_hop[g].wait_send()
+    for gather in gathers:
+        gather.wait_send()
+    for owner, send in sends:
+
+        @pl.when(owner != me)
+        def _():
+            send.wait_send()
+
+    @pl.when(me < sp_devices - 1)
+    def _():
+        to_next.wait_send()
+
+    @pl.when(me > 0)
+    def _():
+        to_previous.wait_send()
+
+
+def routing(route_ids, route_weights, experts, capacity):
+    expert_ids = jnp.arange(experts, dtype=jnp.int32)
+    chosen = route_ids[:, :, None] == expert_ids
+    hit = jnp.any(chosen, axis=1)
+    token_weight = jnp.sum(jnp.where(chosen, route_weights[:, :, None], 0.0), axis=1)
+    tokens_here = route_ids.shape[0]
+    token_ids = jnp.arange(tokens_here, dtype=jnp.int32)
+    below = (token_ids[:, None] < token_ids[None, :]).astype(jnp.bfloat16)
+    rank = lax.dot_general(
+        hit.astype(jnp.bfloat16), below, (((0,), (0,)), ((), ())),
+        preferred_element_type=jnp.float32,
+    )
+    rank = jnp.where(hit.T, rank, -1.0)
+    in_slot = rank[:, None, :] == jnp.arange(capacity, dtype=jnp.float32)[None, :, None]
+    slot_weight = jnp.sum(jnp.where(in_slot, token_weight.T[:, None, :], 0.0), axis=2)
+    pick = in_slot.astype(jnp.bfloat16).reshape(experts * capacity, tokens_here)
+    return pick, slot_weight.reshape(-1, 1)
+
+
+def fused_shards(
+    out_cotangent,
+    stream,
+    route_ids,
+    route_weights,
+    gate_proj,
+    up_proj,
+    down_proj,
+    outer_gate,
+    inner_gate,
+    conv_input,
+    conv_taps,
+    out_proj,
+):
+    f32, bf16 = jnp.float32, jnp.bfloat16
+    n = lax.axis_size("sp")
+    tokens, width = stream.shape
+    units = gate_proj.shape[2]
+    channels = out_proj.shape[1]
+    capacity = 4 * tokens // n
+    slots = n * capacity
+    quarter = width // lax.axis_size("tp")
+    per = width // n
+    pick, slot_weight = routing(route_ids, route_weights, n, capacity)
+    groups = [list(range(i, i + 2)) for i in range(0, n, 2)]
+    vmem = pl.BlockSpec(memory_space=pltpu.VMEM)
+    hbm = pl.BlockSpec(memory_space=pl.ANY)
+    dma = pltpu.SemaphoreType.DMA
+    grads = pl.pallas_call(
+        functools.partial(fused, n, groups),
+        out_shape=[
+            jax.ShapeDtypeStruct((width, units), bf16),
+            jax.ShapeDtypeStruct((width, units), bf16),
+            jax.ShapeDtypeStruct((units, width), bf16),
+            jax.ShapeDtypeStruct((per, channels), f32),
+            jax.ShapeDtypeStruct((tokens, channels), f32),
+            jax.ShapeDtypeStruct((tokens, channels), f32),
+            jax.ShapeDtypeStruct((tokens, channels), f32),
+        ],
+        in_specs=[vmem] * 9 + [hbm] * 3,
+        out_specs=[vmem] * 7,
+        scratch_shapes=[
+            pltpu.VMEM((2, slots, width), bf16),
+            pltpu.VMEM((n - 1, 2, capacity, quarter), bf16),
+            pltpu.VMEM((width, 2 * units), bf16),
+            pltpu.VMEM((units, width), bf16),
+            pltpu.VMEM((slots, units), bf16),
+            pltpu.VMEM((slots, 2 * units), bf16),
+            pltpu.VMEM((2, slots, quarter), bf16),
+            pltpu.VMEM((slots, quarter), f32),
+            pltpu.VMEM((2, slots, quarter), bf16),
+            pltpu.VMEM((2, slots, quarter), bf16),
+            pltpu.VMEM((slots, quarter), bf16),
+            pltpu.VMEM((slots, quarter), bf16),
+            pltpu.VMEM((slots, quarter), bf16),
+            pltpu.VMEM((slots, quarter), bf16),
+            pltpu.VMEM((tokens, width), bf16),
+            pltpu.VMEM((width // quarter, quarter, channels), bf16),
+            pltpu.VMEM((n, per, channels), bf16),
+            pltpu.VMEM((tokens + 8, channels), f32),
+            pltpu.VMEM((tokens + 8, channels), f32),
+            pltpu.VMEM((tokens, channels), f32),
+            pltpu.VMEM((tokens, channels), bf16),
+            dma((3,)),
+            dma((2, n)),
+            dma((2, n)),
+            dma((4, n)),
+            dma((2, 2, len(groups))),
+            dma((2, len(groups))),
+            dma((2, n)),
+            dma((2, 3)),
+            dma((2, n)),
+            dma((4,)),
+        ],
+        compiler_params=pltpu.CompilerParams(
+            collective_id=0, has_side_effects=True, vmem_limit_bytes=60 * 1024 * 1024
+        ),
+    )(
+        out_cotangent,
+        stream,
+        pick,
+        slot_weight,
+        outer_gate,
+        inner_gate,
+        conv_input,
+        conv_taps,
+        out_proj,
+        gate_proj[0],
+        up_proj[0],
+        down_proj[0],
+    )
+    return (grads[0][None], grads[1][None], grads[2][None], *grads[3:])
+
+
+def fits_kernel(mesh):
+    n = mesh.shape["sp"]
+    return mesh.shape["tp"] == 4 and n & (n - 1) == 0 and n <= 8
+
+
 def solution(mesh):
     placed = (
         P("sp", None),
@@ -200,7 +736,7 @@
         P(None, "tp"),
     )
     return jax.shard_map(
-        shards,
+        fused_shards if fits_kernel(mesh) else shards,
         mesh=mesh,
         in_specs=placed,
         out_specs=(

time: 230 us -> 158 us (0.69); the launches traced: 226 us -> 157 us
  Pallas kernels: 0 us -> 144 us
  waiting for transfers between devices: 84.3 us -> 0 us
  blocking collectives: 59.1 us -> 0 us
  matrix products: 31.5 us -> 0.15 us
  starting transfers between devices: 23.9 us -> 0 us
  between operations: 14.1 us -> 0.68 us
  other arithmetic: 9.56 us -> 1.23 us
  local copies, waits for them, and re-layouts: 3.85 us -> 10.7 us
    pallas_call x0 -> x1, Pallas kernels: none -> 144 us  [fused_shards(): pl.pallas_call(functools.partial(fused, n, groups), out_shape=[jax.ShapeD...]
    all_to_all x2 -> x0, blocking collectives: 59.1 us -> none  [to_owners(): lax.all_to_all(blocks, 'sp', split_axis=0, concat_axis=0, tiled=True)]
    all_gather x3 -> x0, waiting for transfers between devices: 44.9 us -> none  [the longest x1 26.2 us: shards(): rows_grad = lax.all_gather(got_grad, 'tp', axis=1, tiled=True)]
    dot_general x21 -> x1, matrix products: 31.5 us -> 0.15 us  [routing(): lax.dot_general(hit.astype(jnp.bfloat16), below, (((0,), (0,)), ((), ()))...]
    ppermute x6 -> x0, waiting for transfers between devices: 23.8 us -> none  [the longest x4 20.3 us: swapped(): return lax.ppermute(x, 'tp', [(i, i ^ flip) for i in range(devices)])]
    all_to_all x3 -> x0, starting transfers between devices: 16.5 us -> none  [to_owners(): lax.all_to_all(blocks, 'sp', split_axis=0, concat_axis=0, tiled=True)]
    all_to_all x3 -> x0, waiting for transfers between devices: 15.5 us -> none  [to_owners(): lax.all_to_all(blocks, 'sp', split_axis=0, concat_axis=0, tiled=True)]
    unnamed x40 -> x23, local copies, waits for them, and re-layouts: 1.9 us -> 9.69 us
  transfers between devices with their start and end apart: 12 -> 0, of which waited for: 8 -> 0; matrix products, arithmetic and copies ran while one was open for 13% -> 0% of each run, Pallas kernels for 0% -> 0%
where the time goes in v1:
time: 158 us; the launch traced here: 157 us
  Pallas kernels  144 us (91%)
  local copies, waits for them, and re-layouts  10.7 us (7%)
    pallas_call x1, Pallas kernels, fused_shards(): pl.pallas_call(functools.partial(fused, n, groups), out_shape=[jax.ShapeD...  144 us
    unnamed x23, local copies, waits for them, and re-layouts  9.69 us

profile of v1, /device:TPU:7, one launch (start us, length us, event | category | flops | bytes accessed | tf_op | source)
XLA Modules:
  0.0 157.2 jit_solution(11080988741210874911)
XLA Ops:
  0.6 0.0 copy-start.6
  0.6 0.7 copy-done.6
  1.3 0.0 copy-start.7
  1.3 0.1 convolution_select_fusion
  1.5 0.5 copy-done.7
  2.0 0.2 select_reduce_fusion
  2.2 1.0 fusion.pick_ref
  3.2 1.0 copy.24.slot_weight_ref
  4.3 144.4 %shard_map.171 = (bf16[2048,256]{1,0:T(8,128)(2,1)}, bf16[2048,256]{1,0:T(8,128)(2,1)}, bf16[256,2048]{1,0:T(8,128)(2,1)}, f32[256,128]{1,0:T(8,128)}, f32[256,1...) custom-call(bf16[256,2048]{1,0:T(8,128)(2,1)} %cot_ref.1, bf16[256,2048]{1,0:T(8,128)(2,1)} %stream_ref.1, ...), custom_call_target="tpu_custom_call" | custom-call | tf_op jit(solution)/shard_map/pallas_call | solution.py:652
  148.7 0.0 copy-start.1
  148.7 2.4 %copy.32 = bf16[1,2048,256]{2,1,0:T(8,128)(2,1)} copy(bf16[1,2048,256]{2,1,0:T(8,128)(2,1)} %bitcast.22) | data formatting | bytes 2097152
  151.0 0.0 copy-done.1
  151.1 0.0 copy-start
  151.1 1.0 copy.33
  152.0 0.6 copy-done
  152.7 0.0 copy-start.5
  152.7 1.0 copy.34
  153.6 0.1 copy-done.5
  153.7 0.0 copy-start.4
  153.7 0.7 copy.35
  154.3 0.3 copy-done.4
  154.6 0.0 copy-start.3
  154.6 0.7 copy.36
  155.3 0.3 copy-done.3
  155.6 0.0 copy-start.2
  155.6 0.7 copy.37
  156.2 0.3 copy-done.2
  156.5 0.7 copy.38
  (3 shorter events, 0.0 us)
Async XLA Ops:
  0.6 0.7 copy-start.6
  1.3 0.7 copy-start.7
  148.7 2.4 %copy-start.1 = (bf16[2048,256]{1,0:T(8,128)(2,1)S(1)}, bf16[2048,256]{1,0:T(8,128)(2,1)}, u32[]{:S(2)}) copy-start(bf16[2048,256]{1,0:T(8,128)(2,1)} %get-tuple-element.15) | copy-start | bytes 3145732
  151.1 1.6 %copy-start = (bf16[256,2048]{1,0:T(8,128)(2,1)S(1)}, bf16[256,2048]{1,0:T(8,128)(2,1)}, u32[]{:S(2)}) copy-start(bf16[256,2048]{1,0:T(8,128)(2,1)} %get-tuple-element.16) | copy-start | bytes 3145732
  152.7 1.0 copy-start.5
  153.7 1.0 copy-start.4
  154.6 1.0 copy-start.3
  155.6 1.0 copy-start.2

commit v2 on v1

--- a/solution.py
+++ b/solution.py
@@ -202,19 +202,21 @@
 
 def fused(
     sp_devices,
+    labels,
+    sending,
     groups,
-    cot_ref,
-    stream_ref,
-    pick_ref,
-    slot_weight_ref,
-    outer_ref,
-    inner_ref,
-    input_ref,
-    taps_ref,
-    out_proj_ref,
-    w_gate_ref,
-    w_up_ref,
-    w_down_ref,
+    cot_hbm,
+    stream_hbm,
+    ids_hbm,
+    weights_hbm,
+    outer_hbm,
+    inner_hbm,
+    input_hbm,
+    taps_hbm,
+    out_proj_hbm,
+    w_gate_hbm,
+    w_up_hbm,
+    w_down_hbm,
     grad_gate_ref,
     grad_up_ref,
     grad_down_ref,
@@ -222,6 +224,18 @@
     grad_outer_ref,
     grad_inner_ref,
     grad_input_ref,
+    cot_ref,
+    stream_ref,
+    ids_ref,
+    weights_ref,
+    outer_ref,
+    inner_ref,
+    input_ref,
+    taps_ref,
+    out_proj_ref,
+    rank_ref,
+    weight_ref,
+    pick_ref,
     rows,
     a_send,
     w_pair,
@@ -255,9 +269,11 @@
     conv_sem,
 ):
     f32, bf16 = jnp.float32, jnp.bfloat16
+    scope = jax.named_scope
     me = lax.axis_index("sp")
     t = lax.axis_index("tp")
-    t_core, t_y, t_far = flipped(t, 1), flipped(t, 2), flipped(t, 3)
+    t_core, t_y = flipped(t, 1), flipped(t, 2)
+    half = lax.axis_size("tp") // 2
     tokens, width = stream_ref.shape
     capacity = pick_ref.shape[0] // sp_devices
     units = hidden.shape[1]
@@ -265,12 +281,21 @@
     per = width // sp_devices
     over_rows = (((0,), (0,)), ((), ()))
     across = (((1,), (1,)), ((), ()))
-
-    def columns(q):
-        return pl.ds(pl.multiple_of(q * quarter, quarter), quarter)
-
-    def block(k):
-        return pl.ds(k * capacity, capacity)
+    others = range(1, sp_devices)
+
+    def owned(member):
+        return (member % 2) * half + member // 2
+
+    q, q_core, q_y, q_far = owned(t), owned(t_core), owned(t_y), owned(flipped(t, 3))
+
+    def columns(index):
+        return pl.ds(pl.multiple_of(index * quarter, quarter), quarter)
+
+    def block(p):
+        return pl.ds(p * capacity, capacity)
+
+    def dynamic_block(p):
+        return pl.ds(pl.multiple_of(p * capacity, capacity), capacity)
 
     def remote(src, dst, sems, sp, tp):
         return pltpu.make_async_remote_copy(
@@ -282,54 +307,95 @@
             device_id_type=MESH,
         )
 
-    peers = [(flipped(me, k), t) for k in range(1, sp_devices)] + [(me, t_core), (me, t_y)]
+    peers = [(flipped(me, k), t) for k in others] + [(me, t_core), (me, t_y)]
     barrier = pltpu.get_barrier_semaphore()
     for peer in peers:
         pl.semaphore_signal(barrier, inc=1, device_id=peer, device_id_type=MESH)
 
+    moved = [
+        (ids_hbm, ids_ref),
+        (weights_hbm, weights_ref),
+        (inner_hbm, inner_ref),
+        (input_hbm, input_ref),
+        (stream_hbm, stream_ref),
+        (cot_hbm, cot_ref),
+        (w_gate_hbm, w_pair.at[:, pl.ds(0, units)]),
+        (w_up_hbm, w_pair.at[:, pl.ds(units, units)]),
+        (w_down_hbm, w_down),
+        (outer_hbm, outer_ref),
+        (taps_hbm, taps_ref),
+        (out_proj_hbm, out_proj_ref),
+    ]
     loads = [
-        pltpu.make_async_copy(w_gate_ref, w_pair.at[:, pl.ds(0, units)], load_sem.at[0]),
-        pltpu.make_async_copy(w_up_ref, w_pair.at[:, pl.ds(units, units)], load_sem.at[1]),
-        pltpu.make_async_copy(w_down_ref, w_down, load_sem.at[2]),
+        pltpu.make_async_copy(src, dst, load_sem.at[i]) for i, (src, dst) in enumerate(moved)
     ]
     for load in loads:
         load.start()
-    mixed = inner_ref[...].astype(f32) * input_ref[...].astype(f32)
-    before[pl.ds(8, tokens), :] = mixed
-
-    pl.semaphore_wait(barrier, len(peers))
-
-    others = range(1, sp_devices)
-    a, b, c_near, c_far, back = {}, {}, {}, {}, {}
-    for k in others:
-        mine, theirs = rows.at[:, block(k), columns(t)], rows.at[:, block(k), columns(t_y)]
-        peer = flipped(me, k)
-        a[k] = remote(a_send.at[k - 1], mine, (a_sem.at[0, k], a_sem.at[1, k]), peer, t)
-        b[k] = remote(mine, mine, (b_sem.at[0, k], b_sem.at[1, k]), me, t_y)
-        c_near[k] = remote(mine, mine, (c_sem.at[0, k], c_sem.at[1, k]), me, t_core)
-        c_far[k] = remote(theirs, theirs, (c_sem.at[2, k], c_sem.at[3, k]), me, t_core)
-        back[k] = remote(
-            back_send.at[block(k)],
-            back_got.at[pl.ds(pl.multiple_of(me * capacity, capacity), capacity)],
-            (back_sem.at[0, k], back_sem.at[1, k]),
-            peer,
+
+    with scope("prep"):
+        for load in loads[:4]:
+            load.wait()
+        before[pl.ds(8, tokens), :] = inner_ref[...].astype(f32) * input_ref[...].astype(f32)
+        expert_ids = lax.broadcasted_iota(jnp.int32, (sp_devices, tokens), 0)
+        chosen = [ids_ref[j : j + 1, :] == expert_ids for j in range(ids_ref.shape[0])]
+        hit = jnp.zeros((sp_devices, tokens), f32)
+        weight = jnp.zeros((sp_devices, tokens), f32)
+        for j, choice in enumerate(chosen):
+            hit = jnp.where(choice, 1.0, hit)
+            weight = jnp.where(choice, weights_ref[j : j + 1, :], weight)
+        earlier = lax.broadcasted_iota(jnp.int32, (tokens, tokens), 0)
+        later = lax.broadcasted_iota(jnp.int32, (tokens, tokens), 1)
+        below = jnp.where(earlier < later, 1.0, 0.0).astype(bf16)
+        rank = jnp.dot(hit.astype(bf16), below, preferred_element_type=f32)
+        rank_ref[...] = jnp.where(hit > 0.0, rank, -1.0)
+        weight_ref[...] = weight
+        slot = lax.broadcasted_iota(jnp.int32, (capacity, tokens), 0).astype(f32)
+
+    def picked(expert):
+        chosen_slot = rank_ref[pl.ds(expert, 1), :] == slot
+        pick = jnp.where(chosen_slot, 1.0, 0.0).astype(bf16)
+        pick_ref[dynamic_block(expert), :] = pick
+        scale = jnp.sum(
+            jnp.where(chosen_slot, weight_ref[pl.ds(expert, 1), :], 0.0), axis=1, keepdims=True
+        )
+        return pick, scale
+
+    def compacted(choice, at):
+        pick, scale = choice
+        return (
+            jnp.dot(pick, stream_ref[:, at], preferred_element_type=f32).astype(bf16),
+            (scale * jnp.dot(pick, cot_ref[:, at], preferred_element_type=f32)).astype(bf16),
+        )
+
+    place = {label: p for p, label in enumerate(labels)}
+    a, a_extra, b, c_near, c_far, back_out, back_in = {}, {}, {}, {}, {}, {}, {}
+    partners = {}
+    for label in others:
+        p = place[label]
+        partner = partners[label] = flipped(me, label)
+        mine, theirs = rows.at[:, block(p), columns(q)], rows.at[:, block(p), columns(q_y)]
+        a[p] = remote(a_send.at[label], mine, (a_sem.at[0, label], a_sem.at[1, p]), partner, t)
+        if label == 1:
+            a_extra[p] = remote(
+                a_send.at[0], theirs, (a_sem.at[0, 0], a_sem.at[1, 0]), partner, t
+            )
+        b[p] = remote(mine, mine, (b_sem.at[0, p], b_sem.at[1, p]), me, t_y)
+        c_near[p] = remote(mine, mine, (c_sem.at[0, p], c_sem.at[1, p]), me, t_core)
+        c_far[p] = remote(theirs, theirs, (c_sem.at[2, p], c_sem.at[3, p]), me, t_core)
+        back_out[p] = remote(
+            back_send.at[block(p)],
+            back_got.at[dynamic_block(me)],
+            (back_sem.at[0, p], back_sem.at[1, p]),
+            partner,
             t,
         )
-
-    def slots_of(k):
-        return pl.ds(pl.multiple_of(flipped(me, k) * capacity, capacity), capacity)
-
-    for k in others:
-        pick = pick_ref[slots_of(k), :]
-        a_send[k - 1, 0] = jnp.dot(
-            pick, stream_ref[:, columns(t)], preferred_element_type=f32
-        ).astype(bf16)
-        a_send[k - 1, 1] = (
-            slot_weight_ref[slots_of(k), :]
-            * jnp.dot(pick, cot_ref[:, columns(t)], preferred_element_type=f32)
-        ).astype(bf16)
-        a[k].start()
-
+        back_in[p] = remote(
+            back_send.at[block(p)],
+            back_got.at[dynamic_block(partner)],
+            (back_sem.at[0, p], back_sem.at[1, p]),
+            partner,
+            t,
+        )
     to_next = remote(
         before.at[pl.ds(tokens, 8)],
         before.at[pl.ds(0, 8)],
@@ -345,68 +411,83 @@
         t,
     )
 
-    @pl.when(me < sp_devices - 1)
-    def _():
-        to_next.start()
-
-    pick = pick_ref[slots_of(0), :]
-    rows[0, block(0), :] = jnp.dot(pick, stream_ref[...], preferred_element_type=f32).astype(bf16)
-    rows[1, block(0), :] = (
-        slot_weight_ref[slots_of(0), :]
-        * jnp.dot(pick, cot_ref[...], preferred_element_type=f32)
-    ).astype(bf16)
-
-    @pl.when(me == 0)
-    def _():
-        before[pl.ds(0, 8), :] = jnp.zeros((8, before.shape[1]), f32)
-
-    @pl.when(me > 0)
-    def _():
-        to_next.wait_recv()
-
-    conv = (
-        taps_ref[0:1, :] * before[pl.ds(6, tokens), :]
-        + taps_ref[1:2, :] * before[pl.ds(7, tokens), :]
-        + taps_ref[2:3, :] * before[pl.ds(8, tokens), :]
-    )
-    conv_out[...] = conv
-    mixer_out[...] = (outer_ref[...].astype(f32) * conv).astype(bf16)
-    for load in loads:
+    with scope("loads"):
+        loads[4].wait()
+        loads[5].wait()
+    first = True
+    for label in sending:
+        p = place[label]
+        choice = picked(partners[label])
+        a_send[label, 0], a_send[label, 1] = compacted(choice, columns(q))
+        if label == 1:
+            a_send[0, 0], a_send[0, 1] = compacted(choice, columns(q_y))
+        if first:
+            first = False
+            with scope("barrier"):
+                pl.semaphore_wait(barrier, len(peers))
+
+            @pl.when(me < sp_devices - 1)
+            def _():
+                to_next.start()
+
+        a[p].start()
+        if label == 1:
+            a_extra[p].start()
+
+    own = compacted(picked(me), pl.ds(0, width))
+    rows[0, block(place[0]), :], rows[1, block(place[0]), :] = own
+    for load in loads[6:]:
         load.wait()
 
     core, y_hop = {}, {}
-    for g, ks in enumerate(groups):
-        span = pl.ds(ks[0] * capacity, len(ks) * capacity)
+
+    def span_of(ps):
+        return pl.ds(ps[0] * capacity, len(ps) * capacity)
+
+    for g, ps in enumerate(groups):
+        span = span_of(ps)
         core[g] = [
             remote(
-                core_send.at[i, span], core_got.at[i, span],
-                (core_sem.at[0, i, g], core_sem.at[1, i, g]), me, t_core,
+                core_send.at[i, span],
+                core_got.at[i, span],
+                (core_sem.at[0, i, g], core_sem.at[1, i, g]),
+                me,
+                t_core,
             )
             for i in range(2)
         ]
-        y_hop[g] = remote(y_send.at[span], y_got.at[span], (y_sem.at[0, g], y_sem.at[1, g]), me, t_y)
-
-    def stage_a(ks):
-        for k in ks:
-            if k:
-                a[k].wait_recv()
-                b[k].start()
-                c_near[k].start()
-
-    def stage_b(ks):
-        for k in ks:
-            if k:
-                b[k].wait_recv()
-                c_far[k].start()
-
-    def stage_c(ks):
-        for k in ks:
-            if k:
-                c_near[k].wait_recv()
-                c_far[k].wait_recv()
-
-    def expert(g, ks):
-        span = pl.ds(ks[0] * capacity, len(ks) * capacity)
+        y_hop[g] = remote(
+            y_send.at[span], y_got.at[span], (y_sem.at[0, g], y_sem.at[1, g]), me, t_y
+        )
+
+    def stage_a(ps):
+        for p in ps:
+            if labels[p]:
+                with scope(f"a{labels[p]}"):
+                    a[p].wait_recv()
+                if p not in a_extra:
+                    b[p].start()
+                c_near[p].start()
+
+    def stage_b(ps):
+        for p in ps:
+            if labels[p]:
+                with scope(f"b{labels[p]}"):
+                    if p in a_extra:
+                        a_extra[p].wait_recv()
+                    else:
+                        b[p].wait_recv()
+                c_far[p].start()
+
+    def stage_c(ps):
+        for p in ps:
+            if labels[p]:
+                with scope(f"c{labels[p]}"):
+                    c_near[p].wait_recv()
+                    c_far[p].wait_recv()
+
+    def expert(g, ps):
+        span = span_of(ps)
         both = jnp.dot(rows[0, span, :], w_pair[...], preferred_element_type=f32)
         gate, up = both[:, :units], both[:, units:]
         d_hidden = lax.dot_general(
@@ -420,21 +501,22 @@
         d_pair[span, pl.ds(0, units)] = d_gate
         d_pair[span, pl.ds(units, units)] = d_up
 
-        def partial(q):
+        def partial(index):
             return lax.dot_general(
-                d_pair[span, :], w_pair[columns(q), :], across, preferred_element_type=f32
+                d_pair[span, :], w_pair[columns(index), :], across, preferred_element_type=f32
             ).astype(bf16)
 
-        core_send[1, span, :] = partial(t_far)
-        core_send[0, span, :] = partial(t_core)
+        core_send[1, span, :] = partial(q_far)
+        core_send[0, span, :] = partial(q_core)
         core[g][1].start()
-        kept[1, span, :] = partial(t_y)
+        kept[1, span, :] = partial(q_y)
         core[g][0].start()
-        kept[0, span, :] = partial(t)
-
-    def reduce_core(g, ks):
-        span = pl.ds(ks[0] * capacity, len(ks) * capacity)
-        core[g][1].wait_recv()
+        kept[0, span, :] = partial(q)
+
+    def reduce_core(g, ps):
+        span = span_of(ps)
+        with scope(f"rcw{g}"):
+            core[g][1].wait_recv()
         y_send[span, :] = (
             kept[1, span, :].astype(f32) + core_got[1, span, :].astype(f32)
         ).astype(bf16)
@@ -442,29 +524,30 @@
         near_got[span, :] = kept[0, span, :].astype(f32) + core_got[0, span, :].astype(f32)
         y_hop[g].start()
 
-    def reduce_y(g, ks):
-        span = pl.ds(ks[0] * capacity, len(ks) * capacity)
-        y_hop[g].wait_recv()
+    def reduce_y(g, ps):
+        span = span_of(ps)
+        with scope(f"ryw{g}"):
+            y_hop[g].wait_recv()
         back_send[span, :] = (near_got[span, :] + y_got[span, :].astype(f32)).astype(bf16)
-        for k in ks:
-            if k:
-                back[k].start()
+        for p in ps:
+            if labels[p]:
+                back_out[p].start()
             else:
-                own = pl.ds(pl.multiple_of(me * capacity, capacity), capacity)
-                back_got[own, :] = back_send[block(0), :]
+                back_got[dynamic_block(me), :] = back_send[block(p), :]
 
     stage_a(groups[0])
     last = len(groups) - 1
-    for g, ks in enumerate(groups):
+    for g, ps in enumerate(groups):
         if g < last:
             stage_a(groups[g + 1])
-        stage_b(ks)
+        stage_b(ps)
         if g:
             reduce_y(g - 1, groups[g - 1])
-        stage_c(ks)
-        expert(g, ks)
+        stage_c(ps)
+        with scope(f"expert{g}"):
+            expert(g, ps)
         if g < last:
-            reduce_core(g, ks)
+            reduce_core(g, ps)
 
     step = 2 * units
 
@@ -484,17 +567,38 @@
         grad_up_ref[at, :] = both[:, units:]
         return carry
 
-    lax.fori_loop(0, width // step, down, 0)
+    with scope("down"):
+        lax.fori_loop(0, width // step, down, 0)
     reduce_core(last, groups[last])
-    lax.fori_loop(0, width // units // 2, gate_up, 0)
+
+    @pl.when(me == 0)
+    def _():
+        before[pl.ds(0, 8), :] = jnp.zeros((8, before.shape[1]), f32)
+
+    @pl.when(me > 0)
+    def _():
+        to_next.wait_recv()
+
+    conv = (
+        taps_ref[0:1, :] * before[pl.ds(6, tokens), :]
+        + taps_ref[1:2, :] * before[pl.ds(7, tokens), :]
+        + taps_ref[2:3, :] * before[pl.ds(8, tokens), :]
+    )
+    conv_out[...] = conv
+    mixer_out[...] = (outer_ref[...].astype(f32) * conv).astype(bf16)
+    with scope("gu1"):
+        lax.fori_loop(0, width // units // 2, gate_up, 0)
     reduce_y(last, groups[last])
-    lax.fori_loop(width // units // 2, width // units, gate_up, 0)
-
-    for k in others:
-        back[k].wait_recv()
+    with scope("gu2"):
+        lax.fori_loop(width // units // 2, width // units, gate_up, 0)
+
+    for p, label in enumerate(labels):
+        if label:
+            with scope(f"back{label}"):
+                back_in[p].wait_recv()
     moe_grad = lax.dot_general(pick_ref[...], back_got[...], over_rows, preferred_element_type=f32)
-    stream_grad[:, columns(t)] = (cot_ref[:, columns(t)].astype(f32) + moe_grad).astype(bf16)
-    part, part_y = stream_grad.at[:, columns(t)], stream_grad.at[:, columns(t_y)]
+    stream_grad[:, columns(q)] = (cot_ref[:, columns(q)].astype(f32) + moe_grad).astype(bf16)
+    part, part_y = stream_grad.at[:, columns(q)], stream_grad.at[:, columns(q_y)]
     gathers = [
         remote(part, part, (gather_sem.at[0, 0], gather_sem.at[1, 0]), me, t_y),
         remote(part, part, (gather_sem.at[0, 1], gather_sem.at[1, 1]), me, t_core),
@@ -505,13 +609,13 @@
     share = quarter // per
     sends = []
 
-    def project(j, q):
-        piece = stream_grad[:, columns(q)]
+    def project(j, index):
+        piece = stream_grad[:, columns(index)]
         proj_send[j] = lax.dot_general(
             piece, mixer_out[...], over_rows, preferred_element_type=f32
         ).astype(bf16)
         for i in range(share):
-            owner = q * share + i
+            owner = index * share + i
             send = remote(
                 proj_send.at[j, pl.ds(i * per, per)],
                 proj_got.at[me],
@@ -529,16 +633,20 @@
                 proj_got[me] = proj_send[j, pl.ds(i * per, per), :]
 
             sends.append((owner, send))
-        return jnp.dot(piece, out_proj_ref[columns(q), :], preferred_element_type=f32)
-
-    d_mixer = project(0, t)
-    gathers[1].wait_recv()
-    d_mixer = d_mixer + project(1, t_core)
-    gathers[0].wait_recv()
+        return jnp.dot(piece, out_proj_ref[columns(index), :], preferred_element_type=f32)
+
+    with scope("p0"):
+        d_mixer = project(0, q)
+    with scope("g1"):
+        gathers[1].wait_recv()
+    d_mixer = d_mixer + project(1, q_core)
+    with scope("g0"):
+        gathers[0].wait_recv()
     gathers[2].start()
-    d_mixer = d_mixer + project(2, t_y)
-    gathers[2].wait_recv()
-    d_mixer = d_mixer + project(3, t_far)
+    d_mixer = d_mixer + project(2, q_y)
+    with scope("g2"):
+        gathers[2].wait_recv()
+    d_mixer = d_mixer + project(3, q_far)
 
     d_conv = d_mixer * outer_ref[...].astype(f32)
     after[pl.ds(0, tokens), :] = d_conv
@@ -552,9 +660,11 @@
     def _():
         after[pl.ds(tokens, 8), :] = jnp.zeros((8, after.shape[1]), f32)
 
-    @pl.when(me < sp_devices - 1)
-    def _():
-        to_previous.wait_recv()
+    with scope("prevw"):
+
+        @pl.when(me < sp_devices - 1)
+        def _():
+            to_previous.wait_recv()
 
     d_mixed = (
         taps_ref[2:3, :] * after[pl.ds(0, tokens), :]
@@ -566,21 +676,26 @@
 
     for k in others:
         source = flipped(me, k)
-        remote(
-            proj_send.at[0, pl.ds(0, per)],
-            proj_got.at[source],
-            (proj_sem.at[0, 0], proj_sem.at[1, source]),
-            source,
-            t,
-        ).wait_recv()
+        with scope(f"pw{k}"):
+            remote(
+                proj_send.at[0, pl.ds(0, per)],
+                proj_got.at[source],
+                (proj_sem.at[0, 0], proj_sem.at[1, source]),
+                source,
+                t,
+            ).wait_recv()
     total = proj_got[0].astype(f32)
     for s in range(1, sp_devices):
         total = total + proj_got[s].astype(f32)
     grad_proj_ref[...] = total
 
-    for k in others:
-        for copy in (a[k], b[k], c_near[k], c_far[k], back[k]):
-            copy.wait_send()
+    for label in others:
+        p = place[label]
+        for copy in (a[p], a_extra.get(p), c_near[p], c_far[p], back_out[p]):
+            if copy is not None:
+                copy.wait_send()
+        if p not in a_extra:
+            b[p].wait_send()
     for g in range(len(groups)):
         core[g][0].wait_send()
         core[g][1].wait_send()
@@ -602,23 +717,16 @@
         to_previous.wait_send()
 
 
-def routing(route_ids, route_weights, experts, capacity):
-    expert_ids = jnp.arange(experts, dtype=jnp.int32)
-    chosen = route_ids[:, :, None] == expert_ids
-    hit = jnp.any(chosen, axis=1)
-    token_weight = jnp.sum(jnp.where(chosen, route_weights[:, :, None], 0.0), axis=1)
-    tokens_here = route_ids.shape[0]
-    token_ids = jnp.arange(tokens_here, dtype=jnp.int32)
-    below = (token_ids[:, None] < token_ids[None, :]).astype(jnp.bfloat16)
-    rank = lax.dot_general(
-        hit.astype(jnp.bfloat16), below, (((0,), (0,)), ((), ())),
-        preferred_element_type=jnp.float32,
-    )
-    rank = jnp.where(hit.T, rank, -1.0)
-    in_slot = rank[:, None, :] == jnp.arange(capacity, dtype=jnp.float32)[None, :, None]
-    slot_weight = jnp.sum(jnp.where(in_slot, token_weight.T[:, None, :], 0.0), axis=2)
-    pick = in_slot.astype(jnp.bfloat16).reshape(experts * capacity, tokens_here)
-    return pick, slot_weight.reshape(-1, 1)
+def written(*refs):
+    count = (len(refs) - 1) // 2
+    sem = refs[-1]
+    outs = [
+        pltpu.make_async_copy(refs[i], refs[count + i], sem.at[i]) for i in range(count)
+    ]
+    for out in outs:
+        out.start()
+    for out in outs:
+        out.wait()
 
 
 def fused_shards(
@@ -644,27 +752,61 @@
     slots = n * capacity
     quarter = width // lax.axis_size("tp")
     per = width // n
-    pick, slot_weight = routing(route_ids, route_weights, n, capacity)
-    groups = [list(range(i, i + 2)) for i in range(0, n, 2)]
+    if n == 8:
+        labels = [0, 2, 3, 6, 7, 1, 4, 5]
+        sending = [2, 3, 6, 7, 4, 5, 1]
+        groups = [[0, 1], [2, 3], [4, 5], [6], [7]]
+    else:
+        labels = list(range(n))
+        sending = labels[1:]
+        groups = [[i] for i in labels]
     vmem = pl.BlockSpec(memory_space=pltpu.VMEM)
-    hbm = pl.BlockSpec(memory_space=pl.ANY)
+    hbm = pl.BlockSpec(memory_space=pltpu.HBM)
+    anywhere = pl.BlockSpec(memory_space=pl.ANY)
     dma = pltpu.SemaphoreType.DMA
+    shapes = [
+        ((width, units), bf16),
+        ((width, units), bf16),
+        ((units, width), bf16),
+        ((per, channels), f32),
+        ((tokens, channels), f32),
+        ((tokens, channels), f32),
+        ((tokens, channels), f32),
+    ]
+    args = (
+        out_cotangent,
+        stream,
+        route_ids.T,
+        route_weights.T,
+        outer_gate,
+        inner_gate,
+        conv_input,
+        conv_taps,
+        out_proj,
+        gate_proj[0],
+        up_proj[0],
+        down_proj[0],
+    )
     grads = pl.pallas_call(
-        functools.partial(fused, n, groups),
-        out_shape=[
-            jax.ShapeDtypeStruct((width, units), bf16),
-            jax.ShapeDtypeStruct((width, units), bf16),
-            jax.ShapeDtypeStruct((units, width), bf16),
-            jax.ShapeDtypeStruct((per, channels), f32),
-            jax.ShapeDtypeStruct((tokens, channels), f32),
-            jax.ShapeDtypeStruct((tokens, channels), f32),
-            jax.ShapeDtypeStruct((tokens, channels), f32),
-        ],
-        in_specs=[vmem] * 9 + [hbm] * 3,
+        functools.partial(fused, n, labels, sending, groups),
+        out_shape=[pltpu.VMEM(*shape) for shape in shapes],
+        in_specs=[hbm] * 12,
         out_specs=[vmem] * 7,
         scratch_shapes=[
+            pltpu.VMEM((tokens, width), bf16),
+            pltpu.VMEM((tokens, width), bf16),
+            pltpu.VMEM(route_ids.shape[::-1], jnp.int32),
+            pltpu.VMEM(route_ids.shape[::-1], f32),
+            pltpu.VMEM((tokens, channels), bf16),
+            pltpu.VMEM((tokens, channels), bf16),
+            pltpu.VMEM((tokens, channels), bf16),
+            pltpu.VMEM(conv_taps.shape, f32),
+            pltpu.VMEM((width, channels), bf16),
+            pltpu.VMEM((n, tokens), f32),
+            pltpu.VMEM((n, tokens), f32),
+            pltpu.VMEM((slots, tokens), bf16),
             pltpu.VMEM((2, slots, width), bf16),
-            pltpu.VMEM((n - 1, 2, capacity, quarter), bf16),
+            pltpu.VMEM((n, 2, capacity, quarter), bf16),
             pltpu.VMEM((width, 2 * units), bf16),
             pltpu.VMEM((units, width), bf16),
             pltpu.VMEM((slots, units), bf16),
@@ -684,7 +826,7 @@
             pltpu.VMEM((tokens + 8, channels), f32),
             pltpu.VMEM((tokens, channels), f32),
             pltpu.VMEM((tokens, channels), bf16),
-            dma((3,)),
+            dma((12,)),
             dma((2, n)),
             dma((2, n)),
             dma((4, n)),
@@ -696,23 +838,18 @@
             dma((4,)),
         ],
         compiler_params=pltpu.CompilerParams(
-            collective_id=0, has_side_effects=True, vmem_limit_bytes=60 * 1024 * 1024
+            collective_id=0, has_side_effects=True, vmem_limit_bytes=48 * 1024 * 1024
         ),
-    )(
-        out_cotangent,
-        stream,
-        pick,
-        slot_weight,
-        outer_gate,
-        inner_gate,
-        conv_input,
-        conv_taps,
-        out_proj,
-        gate_proj[0],
-        up_proj[0],
-        down_proj[0],
-    )
-    return (grads[0][None], grads[1][None], grads[2][None], *grads[3:])
+    )(*(pltpu.with_memory_space_constraint(arg, pltpu.HBM) for arg in args))
+    outs = pl.pallas_call(
+        written,
+        out_shape=[jax.ShapeDtypeStruct(*shape) for shape in shapes],
+        in_specs=[anywhere] * 7,
+        out_specs=[hbm] * 7,
+        scratch_shapes=[dma((7,))],
+        compiler_params=pltpu.CompilerParams(vmem_limit_bytes=1024 * 1024),
+    )(*(pltpu.with_memory_space_constraint(grad, pltpu.VMEM) for grad in grads))
+    return (outs[0][None], outs[1][None], outs[2][None], *outs[3:])
 
 
 def fits_kernel(mesh):

time: 158 us -> 111 us (0.70)
  Pallas kernels: 144 us -> 110 us
  local copies, waits for them, and re-layouts: 10.7 us -> 0 us
    pallas_call x1 -> x2, Pallas kernels: 144 us -> 110 us  [the longest x1 108 us: fused_shards(): pl.pallas_call(functools.partial(fused, n, labels, sending, groups), out_...]
    unnamed x23 -> x0, local copies, waits for them, and re-layouts: 9.69 us -> none
where the time goes in v2:
time: 111 us
  Pallas kernels  110 us (99%)
    pallas_call x1, Pallas kernels, fused_shards(): pl.pallas_call(functools.partial(fused, n, labels, sending, groups), out_...  108 us

profile of v2, /device:TPU:7, one launch (start us, length us, event | category | flops | bytes accessed | tf_op | source)
XLA Modules:
  0.0 110.8 jit_solution(10429944380337427514)
XLA Ops:
  0.6 108.3 %shard_map.171 = (bf16[2048,256]{1,0:T(8,128)(2,1)S(1)}, bf16[2048,256]{1,0:T(8,128)(2,1)S(1)}, bf16[256,2048]{1,0:T(8,128)(2,1)S(1)}, f32[256,128]{1,0:T(8,128)...) custom-call(bf16[256,2048]{1,0:T(8,128)(2,1)} %cot_hbm.1, ...), custom_call_target="tpu_custom_call" | custom-call | tf_op jit(solution)/shard_map/pallas_call | solution.py:790
  109.0 1.9 %shard_map.172 = (bf16[2048,256]{1,0:T(8,128)(2,1)}, bf16[2048,256]{1,0:T(8,128)(2,1)}, bf16[256,2048]{1,0:T(8,128)(2,1)}, f32[256,128]{1,0:T(8,128)}, f32[256,1...) custom-call(bf16[2048,256]{1,0:T(8,128)(2,1)S(1)} %get-tuple-element.21.refs_0_, ...), custom_call_target="tpu_custom_call" | custom-call | tf_op jit(solution)/shard_map/pallas_call | solution.py:844

commit v3 on v2

--- a/solution.py
+++ b/solution.py
@@ -203,8 +203,8 @@
 def fused(
     sp_devices,
     labels,
-    sending,
-    groups,
+    outer_steps,
+    inner_steps,
     cot_hbm,
     stream_hbm,
     ids_hbm,
@@ -233,11 +233,14 @@
     input_ref,
     taps_ref,
     out_proj_ref,
-    rank_ref,
-    weight_ref,
+    route,
+    far_route,
+    far_pick,
     pick_ref,
+    raw,
     rows,
     a_send,
+    close_send,
     w_pair,
     w_down,
     hidden,
@@ -258,6 +261,9 @@
     conv_out,
     mixer_out,
     load_sem,
+    route_sem,
+    raw_sem,
+    close_sem,
     a_sem,
     b_sem,
     c_sem,
@@ -347,55 +353,141 @@
         later = lax.broadcasted_iota(jnp.int32, (tokens, tokens), 1)
         below = jnp.where(earlier < later, 1.0, 0.0).astype(bf16)
         rank = jnp.dot(hit.astype(bf16), below, preferred_element_type=f32)
-        rank_ref[...] = jnp.where(hit > 0.0, rank, -1.0)
-        weight_ref[...] = weight
+        route[0] = jnp.where(hit > 0.0, rank, -1.0)
+        route[1] = weight
         slot = lax.broadcasted_iota(jnp.int32, (capacity, tokens), 0).astype(f32)
 
-    def picked(expert):
-        chosen_slot = rank_ref[pl.ds(expert, 1), :] == slot
-        pick = jnp.where(chosen_slot, 1.0, 0.0).astype(bf16)
+    def slots_of(ref, expert):
+        return ref[0, pl.ds(expert, 1), :] == slot
+
+    def one_hot(chosen_slot):
+        return jnp.where(chosen_slot, 1.0, 0.0).astype(bf16)
+
+    def scale_of(ref, expert, chosen_slot):
+        return jnp.sum(
+            jnp.where(chosen_slot, ref[1, pl.ds(expert, 1), :], 0.0), axis=1, keepdims=True
+        )
+
+    def compacted(expert, ranges):
+        chosen_slot = slots_of(route, expert)
+        pick = one_hot(chosen_slot)
         pick_ref[dynamic_block(expert), :] = pick
-        scale = jnp.sum(
-            jnp.where(chosen_slot, weight_ref[pl.ds(expert, 1), :], 0.0), axis=1, keepdims=True
-        )
-        return pick, scale
-
-    def compacted(choice, at):
-        pick, scale = choice
-        return (
-            jnp.dot(pick, stream_ref[:, at], preferred_element_type=f32).astype(bf16),
-            (scale * jnp.dot(pick, cot_ref[:, at], preferred_element_type=f32)).astype(bf16),
-        )
-
+        scale = scale_of(route, expert, chosen_slot)
+        return [
+            (
+                jnp.dot(pick, stream_ref[:, at], preferred_element_type=f32).astype(bf16),
+                (scale * jnp.dot(pick, cot_ref[:, at], preferred_element_type=f32)).astype(bf16),
+            )
+            for at in ranges
+        ]
+
+    z, side = me // 2, me % 2
+    upper = z // 2
+    inside = (z + upper) % 2
+    across_x, near, opposite = flipped(me, 1), flipped(me, 2), flipped(me, 6)
+    lines = [z, z + 1 - 2 * (z % 2), 2 - upper, 3 - 3 * upper]
     place = {label: p for p, label in enumerate(labels)}
-    a, a_extra, b, c_near, c_far, back_out, back_in = {}, {}, {}, {}, {}, {}, {}
-    partners = {}
-    for label in others:
+    a, a_extra, b, c_near, c_far, back_out, back_in, partners = {}, {}, {}, {}, {}, {}, {}, {}
+    for label in range(sp_devices):
         p = place[label]
-        partner = partners[label] = flipped(me, label)
-        mine, theirs = rows.at[:, block(p), columns(q)], rows.at[:, block(p), columns(q_y)]
-        a[p] = remote(a_send.at[label], mine, (a_sem.at[0, label], a_sem.at[1, p]), partner, t)
-        if label == 1:
-            a_extra[p] = remote(
-                a_send.at[0], theirs, (a_sem.at[0, 0], a_sem.at[1, 0]), partner, t
+        across_side = 1 - side if label % 2 else side
+        partner = partners[p] = 2 * lines[label // 2] + across_side
+        a[p], a_extra[p], b[p], c_near[p], c_far[p] = [], [], [], [], []
+        for i in range(2):
+            mine, theirs = rows.at[i, block(p), columns(q)], rows.at[i, block(p), columns(q_y)]
+            if label % 2:
+                a[p].append(
+                    remote(
+                        a_send.at[label // 2, i],
+                        mine,
+                        (a_sem.at[0, i, p], a_sem.at[1, i, p]),
+                        across_x,
+                        t,
+                    )
+                )
+            if label == 1:
+                a_extra[p].append(
+                    remote(
+                        a_send.at[sp_devices // 2, i],
+                        theirs,
+                        (a_sem.at[0, i, 0], a_sem.at[1, i, 0]),
+                        across_x,
+                        t,
+                    )
+                )
+            b[p].append(remote(mine, mine, (b_sem.at[0, i, p], b_sem.at[1, i, p]), me, t_y))
+            c_near[p].append(
+                remote(mine, mine, (c_sem.at[0, i, p], c_sem.at[1, i, p]), me, t_core)
             )
-        b[p] = remote(mine, mine, (b_sem.at[0, p], b_sem.at[1, p]), me, t_y)
-        c_near[p] = remote(mine, mine, (c_sem.at[0, p], c_sem.at[1, p]), me, t_core)
-        c_far[p] = remote(theirs, theirs, (c_sem.at[2, p], c_sem.at[3, p]), me, t_core)
+            c_far[p].append(
+                remote(theirs, theirs, (c_sem.at[2, i, p], c_sem.at[3, i, p]), me, t_core)
+            )
         back_out[p] = remote(
             back_send.at[block(p)],
             back_got.at[dynamic_block(me)],
-            (back_sem.at[0, p], back_sem.at[1, p]),
+            (back_sem.at[0, p], back_sem.at[1, me]),
             partner,
             t,
         )
         back_in[p] = remote(
             back_send.at[block(p)],
             back_got.at[dynamic_block(partner)],
-            (back_sem.at[0, p], back_sem.at[1, p]),
+            (back_sem.at[0, p], back_sem.at[1, partner]),
             partner,
             t,
         )
+    close = [
+        [
+            remote(
+                close_send.at[j, i],
+                rows.at[i, block(place[2 + j]), columns(q)],
+                (close_sem.at[j, i], a_sem.at[1, i, place[2 + j]]),
+                flipped(me, 2 + j),
+                t,
+            )
+            for i in range(2)
+        ]
+        for j in range(2)
+    ]
+    to_near, to_opposite, on_opposite, on_near = [], [], [], [[], []]
+    for i, ref in enumerate((stream_ref, cot_ref)):
+        own = ref.at[:, columns(q)]
+        to_near.append(
+            remote(own, raw.at[0, i], (raw_sem.at[0, i], raw_sem.at[5, i]), near, t)
+        )
+        to_opposite.append(
+            remote(own, raw.at[1, i], (raw_sem.at[1, i], raw_sem.at[6, i]), opposite, t)
+        )
+        on_opposite.append(
+            remote(raw.at[0, i], raw.at[2, i], (raw_sem.at[2, i], raw_sem.at[7, i]), opposite, t)
+        )
+        for j in range(2):
+            on_near[j].append(
+                remote(
+                    raw.at[1 + j, i],
+                    raw.at[1 + j, i],
+                    (raw_sem.at[3 + j, i], raw_sem.at[6 + j, i]),
+                    near,
+                    t,
+                )
+            )
+    as_far = 2 - inside
+    route_out = [
+        remote(route, far_route.at[0], (route_sem.at[0, 0], route_sem.at[1, 0]), near, t)
+    ] + [
+        remote(
+            route,
+            far_route.at[as_far],
+            (route_sem.at[0, j], route_sem.at[1, as_far]),
+            flipped(me, 2 + 2 * j),
+            t,
+        )
+        for j in (1, 2)
+    ]
+    route_in = [
+        remote(route, far_route.at[j], (route_sem.at[0, j], route_sem.at[1, j]), near, t)
+        for j in range(3)
+    ]
     to_next = remote(
         before.at[pl.ds(tokens, 8)],
         before.at[pl.ds(0, 8)],
@@ -411,83 +503,145 @@
         t,
     )
 
-    with scope("loads"):
-        loads[4].wait()
-        loads[5].wait()
-    first = True
-    for label in sending:
-        p = place[label]
-        choice = picked(partners[label])
-        a_send[label, 0], a_send[label, 1] = compacted(choice, columns(q))
-        if label == 1:
-            a_send[0, 0], a_send[0, 1] = compacted(choice, columns(q_y))
-        if first:
-            first = False
-            with scope("barrier"):
-                pl.semaphore_wait(barrier, len(peers))
-
-            @pl.when(me < sp_devices - 1)
-            def _():
-                to_next.start()
-
-        a[p].start()
-        if label == 1:
-            a_extra[p].start()
-
-    own = compacted(picked(me), pl.ds(0, width))
+    with scope("barrier"):
+        pl.semaphore_wait(barrier, len(peers))
+    for out in route_out:
+        out.start()
+
+    @pl.when(me < sp_devices - 1)
+    def _():
+        to_next.start()
+
+    for i in range(2):
+        loads[4 + i].wait()
+
+        @pl.when(inside == 0)
+        def _():
+            to_near[i].start()
+
+        @pl.when(inside == 1)
+        def _():
+            to_opposite[i].start()
+
+    @pl.when(inside == 1)
+    def _():
+        for j in range(2):
+            close_send[j, 0], close_send[j, 1] = compacted(flipped(me, 2 + j), [columns(q)])[0]
+            for i in range(2):
+                close[j][i].start()
+
+    own = compacted(me, [pl.ds(0, width)])[0]
     rows[0, block(place[0]), :], rows[1, block(place[0]), :] = own
     for load in loads[6:]:
         load.wait()
 
     core, y_hop = {}, {}
-
-    def span_of(ps):
-        return pl.ds(ps[0] * capacity, len(ps) * capacity)
-
-    for g, ps in enumerate(groups):
-        span = span_of(ps)
-        core[g] = [
+    for p in range(len(labels)):
+        core[p] = [
             remote(
-                core_send.at[i, span],
-                core_got.at[i, span],
-                (core_sem.at[0, i, g], core_sem.at[1, i, g]),
+                core_send.at[i, block(p)],
+                core_got.at[i, block(p)],
+                (core_sem.at[0, i, p], core_sem.at[1, i, p]),
                 me,
                 t_core,
             )
             for i in range(2)
         ]
-        y_hop[g] = remote(
-            y_send.at[span], y_got.at[span], (y_sem.at[0, g], y_sem.at[1, g]), me, t_y
-        )
-
-    def stage_a(ps):
-        for p in ps:
-            if labels[p]:
-                with scope(f"a{labels[p]}"):
-                    a[p].wait_recv()
-                if p not in a_extra:
-                    b[p].start()
-                c_near[p].start()
-
-    def stage_b(ps):
-        for p in ps:
-            if labels[p]:
-                with scope(f"b{labels[p]}"):
-                    if p in a_extra:
-                        a_extra[p].wait_recv()
-                    else:
-                        b[p].wait_recv()
-                c_far[p].start()
-
-    def stage_c(ps):
-        for p in ps:
-            if labels[p]:
-                with scope(f"c{labels[p]}"):
-                    c_near[p].wait_recv()
-                    c_far[p].wait_recv()
-
-    def expert(g, ps):
-        span = span_of(ps)
+        y_hop[p] = remote(
+            y_send.at[block(p)], y_got.at[block(p)], (y_sem.at[0, p], y_sem.at[1, p]), me, t_y
+        )
+
+    def compact_far(line, i):
+        far = far_route.at[line - 1]
+        if i == 0:
+            route_in[line - 1].wait_recv()
+        for j, expert in enumerate((me, across_x)):
+            chosen_slot = slots_of(far, expert)
+            if i == 0:
+                pick = one_hot(chosen_slot)
+                far_pick[line - 1, j] = pick
+            else:
+                pick = far_pick[line - 1, j]
+            part = jnp.dot(pick, raw[line - 1, i], preferred_element_type=f32)
+            if i:
+                part = scale_of(far, expert, chosen_slot) * part
+            p = place[2 * line + j]
+            if j:
+                a_send[line, i] = part.astype(bf16)
+                a[p][i].start()
+            else:
+                rows[i, block(p), columns(q)] = part.astype(bf16)
+                b[p][i].start()
+                c_near[p][i].start()
+
+    def first_line(i):
+        def go(_):
+            to_near[i].wait_recv()
+            on_opposite[i].start()
+            to_opposite[i].wait_recv()
+            on_near[0][i].start()
+            compact_far(1, i)
+
+        return go
+
+    def relay(i):
+        def go(_):
+            on_opposite[i].wait_recv()
+            on_near[1][i].start()
+
+        return go
+
+    def later_line(line, i, waits):
+        def go(_):
+            if waits:
+                on_near[line - 2][i].wait_recv()
+            compact_far(line, i)
+
+        return go
+
+    def to_side(_):
+        p = place[1]
+        both = compacted(across_x, [columns(q), columns(q_y)])
+        a_send[0, 0], a_send[0, 1] = both[0]
+        a_send[sp_devices // 2, 0], a_send[sp_devices // 2, 1] = both[1]
+        for i in range(2):
+            a[p][i].start()
+
+    def to_side_more(_):
+        for copy in a_extra[place[1]]:
+            copy.start()
+
+    def other_picks(_):
+        for k in range(2, sp_devices):
+            expert = flipped(me, k)
+            pick_ref[dynamic_block(expert), :] = one_hot(slots_of(route, expert))
+
+    def arrive(i):
+        def go(p):
+            (a[p] or close[0])[i].wait_recv()
+            if labels[p] != 1:
+                b[p][i].start()
+            c_near[p][i].start()
+
+        return go
+
+    def cross(i):
+        def go(p):
+            if labels[p] == 1:
+                a_extra[p][i].wait_recv()
+            else:
+                b[p][i].wait_recv()
+            c_far[p][i].start()
+
+        return go
+
+    def gather(p):
+        for i in range(2):
+            c_near[p][i].wait_recv()
+            c_far[p][i].wait_recv()
+
+    def expert(p):
+        span = block(p)
         both = jnp.dot(rows[0, span, :], w_pair[...], preferred_element_type=f32)
         gate, up = both[:, :units], both[:, units:]
         d_hidden = lax.dot_general(
@@ -508,46 +662,46 @@
 
         core_send[1, span, :] = partial(q_far)
         core_send[0, span, :] = partial(q_core)
-        core[g][1].start()
+        core[p][1].start()
         kept[1, span, :] = partial(q_y)
-        core[g][0].start()
+        core[p][0].start()
         kept[0, span, :] = partial(q)
 
-    def reduce_core(g, ps):
-        span = span_of(ps)
-        with scope(f"rcw{g}"):
-            core[g][1].wait_recv()
+    def reduce_core(p):
+        span = block(p)
+        core[p][1].wait_recv()
         y_send[span, :] = (
             kept[1, span, :].astype(f32) + core_got[1, span, :].astype(f32)
         ).astype(bf16)
-        core[g][0].wait_recv()
+        y_hop[p].start()
+        core[p][0].wait_recv()
         near_got[span, :] = kept[0, span, :].astype(f32) + core_got[0, span, :].astype(f32)
-        y_hop[g].start()
-
-    def reduce_y(g, ps):
-        span = span_of(ps)
-        with scope(f"ryw{g}"):
-            y_hop[g].wait_recv()
+
+    def reduce_y(p):
+        span = block(p)
+        y_hop[p].wait_recv()
         back_send[span, :] = (near_got[span, :] + y_got[span, :].astype(f32)).astype(bf16)
-        for p in ps:
-            if labels[p]:
-                back_out[p].start()
-            else:
-                back_got[dynamic_block(me), :] = back_send[block(p), :]
-
-    stage_a(groups[0])
-    last = len(groups) - 1
-    for g, ps in enumerate(groups):
-        if g < last:
-            stage_a(groups[g + 1])
-        stage_b(ps)
-        if g:
-            reduce_y(g - 1, groups[g - 1])
-        stage_c(ps)
-        with scope(f"expert{g}"):
-            expert(g, ps)
-        if g < last:
-            reduce_core(g, ps)
+        if labels[p]:
+            back_out[p].start()
+        else:
+            back_got[dynamic_block(me), :] = back_send[span, :]
+
+    def convolve(p):
+        @pl.when(me == 0)
+        def _():
+            before[pl.ds(0, 8), :] = jnp.zeros((8, before.shape[1]), f32)
+
+        @pl.when(me > 0)
+        def _():
+            to_next.wait_recv()
+
+        conv = (
+            taps_ref[0:1, :] * before[pl.ds(6, tokens), :]
+            + taps_ref[1:2, :] * before[pl.ds(7, tokens), :]
+            + taps_ref[2:3, :] * before[pl.ds(8, tokens), :]
+        )
+        conv_out[...] = conv
+        mixer_out[...] = (outer_ref[...].astype(f32) * conv).astype(bf16)
 
     step = 2 * units
 
@@ -567,86 +721,125 @@
         grad_up_ref[at, :] = both[:, units:]
         return carry
 
-    with scope("down"):
+    def first_gate_up(p):
+        lax.fori_loop(0, width // units // 2, gate_up, 0)
+
+    def second_gate_up(p):
+        lax.fori_loop(width // units // 2, width // units, gate_up, 0)
+
+    def all_down(p):
         lax.fori_loop(0, width // step, down, 0)
-    reduce_core(last, groups[last])
-
-    @pl.when(me == 0)
+
+    def follow(steps, waits):
+        run = dict(
+            a=arrive(0),
+            A=arrive(1),
+            b=cross(0),
+            B=cross(1),
+            C=gather,
+            E=expert,
+            R=reduce_core,
+            Y=reduce_y,
+            V=convolve,
+            G=first_gate_up,
+            H=second_gate_up,
+            D=all_down,
+            w=first_line(0),
+            W=first_line(1),
+            X=to_side,
+            Z=to_side_more,
+            P=other_picks,
+            J=later_line(2, 0, waits),
+            K=later_line(2, 1, waits),
+            L=later_line(3, 0, waits),
+            M=later_line(3, 1, waits),
+            S=relay(0),
+            T=relay(1),
+        )
+        for item in steps.split():
+            with scope(item):
+                run[item[0]](place.get(int(item[1:] or 0)))
+
+    @pl.when(inside == 0)
     def _():
-        before[pl.ds(0, 8), :] = jnp.zeros((8, before.shape[1]), f32)
-
-    @pl.when(me > 0)
+        follow(outer_steps, True)
+
+    @pl.when(inside == 1)
     def _():
-        to_next.wait_recv()
-
-    conv = (
-        taps_ref[0:1, :] * before[pl.ds(6, tokens), :]
-        + taps_ref[1:2, :] * before[pl.ds(7, tokens), :]
-        + taps_ref[2:3, :] * before[pl.ds(8, tokens), :]
-    )
-    conv_out[...] = conv
-    mixer_out[...] = (outer_ref[...].astype(f32) * conv).astype(bf16)
-    with scope("gu1"):
-        lax.fori_loop(0, width // units // 2, gate_up, 0)
-    reduce_y(last, groups[last])
-    with scope("gu2"):
-        lax.fori_loop(width // units // 2, width // units, gate_up, 0)
+        follow(inner_steps, False)
 
     for p, label in enumerate(labels):
         if label:
             with scope(f"back{label}"):
                 back_in[p].wait_recv()
-    moe_grad = lax.dot_general(pick_ref[...], back_got[...], over_rows, preferred_element_type=f32)
-    stream_grad[:, columns(q)] = (cot_ref[:, columns(q)].astype(f32) + moe_grad).astype(bf16)
-    part, part_y = stream_grad.at[:, columns(q)], stream_grad.at[:, columns(q_y)]
-    gathers = [
-        remote(part, part, (gather_sem.at[0, 0], gather_sem.at[1, 0]), me, t_y),
-        remote(part, part, (gather_sem.at[0, 1], gather_sem.at[1, 1]), me, t_core),
-        remote(part_y, part_y, (gather_sem.at[0, 2], gather_sem.at[1, 2]), me, t_core),
-    ]
-    gathers[0].start()
-    gathers[1].start()
     share = quarter // per
+
+    def piece_of(index, i):
+        return pl.ds(pl.multiple_of(index * quarter + i * per, per), per)
+
+    gathers = []
+    for i in range(share):
+        part, part_y = stream_grad.at[:, piece_of(q, i)], stream_grad.at[:, piece_of(q_y, i)]
+        gathers.append(
+            [
+                remote(part, part, (gather_sem.at[0, 0, i], gather_sem.at[1, 0, i]), me, t_y),
+                remote(part, part, (gather_sem.at[0, 1, i], gather_sem.at[1, 1, i]), me, t_core),
+                remote(part_y, part_y, (gather_sem.at[0, 2, i], gather_sem.at[1, 2, i]), me, t_core),
+            ]
+        )
     sends = []
 
-    def project(j, index):
-        piece = stream_grad[:, columns(index)]
-        proj_send[j] = lax.dot_general(
+    def project(j, index, i):
+        piece = stream_grad[:, piece_of(index, i)]
+        proj_send[j * share + i] = lax.dot_general(
             piece, mixer_out[...], over_rows, preferred_element_type=f32
         ).astype(bf16)
-        for i in range(share):
-            owner = index * share + i
-            send = remote(
-                proj_send.at[j, pl.ds(i * per, per)],
-                proj_got.at[me],
-                (proj_sem.at[0, j * share + i], proj_sem.at[1, me]),
-                owner,
-                t,
-            )
-
-            @pl.when(owner != me)
-            def _():
-                send.start()
-
-            @pl.when(owner == me)
-            def _():
-                proj_got[me] = proj_send[j, pl.ds(i * per, per), :]
-
-            sends.append((owner, send))
-        return jnp.dot(piece, out_proj_ref[columns(index), :], preferred_element_type=f32)
-
-    with scope("p0"):
-        d_mixer = project(0, q)
-    with scope("g1"):
-        gathers[1].wait_recv()
-    d_mixer = d_mixer + project(1, q_core)
-    with scope("g0"):
-        gathers[0].wait_recv()
-    gathers[2].start()
-    d_mixer = d_mixer + project(2, q_y)
-    with scope("g2"):
-        gathers[2].wait_recv()
-    d_mixer = d_mixer + project(3, q_far)
+        owner = index * share + i
+        send = remote(
+            proj_send.at[j * share + i],
+            proj_got.at[me],
+            (proj_sem.at[0, j * share + i], proj_sem.at[1, me]),
+            owner,
+            t,
+        )
+
+        @pl.when(owner != me)
+        def _():
+            send.start()
+
+        @pl.when(owner == me)
+        def _():
+            proj_got[me] = proj_send[j * share + i]
+
+        sends.append((owner, send))
+        return jnp.dot(piece, out_proj_ref[piece_of(index, i), :], preferred_element_type=f32)
+
+    for i in range(share):
+        at = piece_of(q, i)
+        moe_grad = lax.dot_general(
+            pick_ref[...],
+            back_got[:, pl.ds(i * per, per)],
+            over_rows,
+            preferred_element_type=f32,
+        )
+        stream_grad[:, at] = (cot_ref[:, at].astype(f32) + moe_grad).astype(bf16)
+        gathers[i][0].start()
+        gathers[i][1].start()
+    d_mixer = project(0, q, 0)
+    for i in range(1, share):
+        d_mixer = d_mixer + project(0, q, i)
+    for i in range(share):
+        with scope(f"g1{i}"):
+            gathers[i][1].wait_recv()
+        d_mixer = d_mixer + project(1, q_core, i)
+    for i in range(share):
+        with scope(f"g0{i}"):
+            gathers[i][0].wait_recv()
+        gathers[i][2].start()
+        d_mixer = d_mixer + project(2, q_y, i)
+        with scope(f"g2{i}"):
+            gathers[i][2].wait_recv()
+        d_mixer = d_mixer + project(3, q_far, i)
 
     d_conv = d_mixer * outer_ref[...].astype(f32)
     after[pl.ds(0, tokens), :] = d_conv
@@ -678,7 +871,7 @@
         source = flipped(me, k)
         with scope(f"pw{k}"):
             remote(
-                proj_send.at[0, pl.ds(0, per)],
+                proj_send.at[0],
                 proj_got.at[source],
                 (proj_sem.at[0, 0], proj_sem.at[1, source]),
                 source,
@@ -691,17 +884,34 @@
 
     for label in others:
         p = place[label]
-        for copy in (a[p], a_extra.get(p), c_near[p], c_far[p], back_out[p]):
-            if copy is not None:
-                copy.wait_send()
-        if p not in a_extra:
-            b[p].wait_send()
-    for g in range(len(groups)):
-        core[g][0].wait_send()
-        core[g][1].wait_send()
-        y_hop[g].wait_send()
-    for gather in gathers:
-        gather.wait_send()
+        for copy in (a[p] if label != 3 else []) + a_extra[p] + c_near[p] + c_far[p]:
+            copy.wait_send()
+        for copy in b[p] if label > 1 else []:
+            copy.wait_send()
+        back_out[p].wait_send()
+    for copy in route_out:
+        copy.wait_send()
+
+    @pl.when(inside == 0)
+    def _():
+        for copy in to_near:
+            copy.wait_send()
+        route_in[0].wait_recv()
+
+    @pl.when(inside == 1)
+    def _():
+        for copy in a[place[3]] + to_opposite + on_opposite + on_near[0] + on_near[1]:
+            copy.wait_send()
+        for copy in close[0] + close[1]:
+            copy.wait_send()
+
+    for p in range(len(labels)):
+        core[p][0].wait_send()
+        core[p][1].wait_send()
+        y_hop[p].wait_send()
+    for copies in gathers:
+        for copy in copies:
+            copy.wait_send()
     for owner, send in sends:
 
         @pl.when(owner != me)
@@ -752,14 +962,17 @@
     slots = n * capacity
     quarter = width // lax.axis_size("tp")
     per = width // n
-    if n == 8:
-        labels = [0, 2, 3, 6, 7, 1, 4, 5]
-        sending = [2, 3, 6, 7, 4, 5, 1]
-        groups = [[0, 1], [2, 3], [4, 5], [6], [7]]
-    else:
-        labels = list(range(n))
-        sending = labels[1:]
-        groups = [[i] for i in labels]
+    labels = [0, 1, 2, 3, 4, 5, 6, 7]
+    outer_steps = (
+        "X Z E0 R0 a2 A2 b2 a3 B2 A3 C2 E2 R2 J Y0 V P b3 B3 C3 E3 R3 K Y2 a1 A1 a5 b1 B1 C1 E1"
+        " L A5 b4 B4 C4 E4 R4 a7 M Y3 b5 B5 C5 E5 R5 Y4 A7 R1 b6 B6 C6 E6 R6 Y5 Y1"
+        " b7 B7 C7 E7 R7 Y6 Y7 G H D"
+    )
+    inner_steps = (
+        "E0 R0 w J W K X a3 a5 b2 B2 S L A3 A5 C2 E2 R2 Y0 V P T M Z b4 B4 C4 E4 R4 a7"
+        " b3 B3 C3 E3 R3 Y2 A7 b5 B5 C5 E5 R5 Y4 a1 A1 b6 B6 C6 E6 R6 Y3 b1 B1 C1 E1 R1 Y5"
+        " b7 B7 C7 E7 R7 Y6 Y1 Y7 G H D"
+    )
     vmem = pl.BlockSpec(memory_space=pltpu.VMEM)
     hbm = pl.BlockSpec(memory_space=pltpu.HBM)
     anywhere = pl.BlockSpec(memory_space=pl.ANY)
@@ -788,7 +1001,7 @@
         down_proj[0],
     )
     grads = pl.pallas_call(
-        functools.partial(fused, n, labels, sending, groups),
+        functools.partial(fused, n, labels, outer_steps, inner_steps),
         out_shape=[pltpu.VMEM(*shape) for shape in shapes],
         in_specs=[hbm] * 12,
         out_specs=[vmem] * 7,
@@ -802,11 +1015,14 @@
             pltpu.VMEM((tokens, channels), bf16),
             pltpu.VMEM(conv_taps.shape, f32),
             pltpu.VMEM((width, channels), bf16),
-            pltpu.VMEM((n, tokens), f32),
-            pltpu.VMEM((n, tokens), f32),
+            pltpu.VMEM((2, n, tokens), f32),
+            pltpu.VMEM((3, 2, n, tokens), f32),
+            pltpu.VMEM((3, 2, capacity, tokens), bf16),
             pltpu.VMEM((slots, tokens), bf16),
+            pltpu.VMEM((3, 2, tokens, quarter), bf16),
             pltpu.VMEM((2, slots, width), bf16),
-            pltpu.VMEM((n, 2, capacity, quarter), bf16),
+            pltpu.VMEM((n // 2 + 1, 2, capacity, quarter), bf16),
+            pltpu.VMEM((2, 2, capacity, quarter), bf16),
             pltpu.VMEM((width, 2 * units), bf16),
             pltpu.VMEM((units, width), bf16),
             pltpu.VMEM((slots, units), bf16),
@@ -820,20 +1036,23 @@
             pltpu.VMEM((slots, quarter), bf16),
             pltpu.VMEM((slots, quarter), bf16),
             pltpu.VMEM((tokens, width), bf16),
-            pltpu.VMEM((width // quarter, quarter, channels), bf16),
+            pltpu.VMEM((n, per, channels), bf16),
             pltpu.VMEM((n, per, channels), bf16),
             pltpu.VMEM((tokens + 8, channels), f32),
             pltpu.VMEM((tokens + 8, channels), f32),
             pltpu.VMEM((tokens, channels), f32),
             pltpu.VMEM((tokens, channels), bf16),
             dma((12,)),
+            dma((2, 3)),
+            dma((8, 2)),
+            dma((2, 2)),
+            dma((2, 2, n)),
+            dma((2, 2, n)),
+            dma((4, 2, n)),
+            dma((2, 2, n)),
             dma((2, n)),
             dma((2, n)),
-            dma((4, n)),
-            dma((2, 2, len(groups))),
-            dma((2, len(groups))),
-            dma((2, n)),
-            dma((2, 3)),
+            dma((2, 3, quarter // per)),
             dma((2, n)),
             dma((4,)),
         ],
@@ -853,8 +1072,7 @@
 
 
 def fits_kernel(mesh):
-    n = mesh.shape["sp"]
-    return mesh.shape["tp"] == 4 and n & (n - 1) == 0 and n <= 8
+    return mesh.shape["sp"] == 8 and mesh.shape["tp"] == 4
 
 
 def solution(mesh):

time: 111 us -> 97.9 us (0.88)
  Pallas kernels: 110 us -> 96.7 us
    pallas_call x1, Pallas kernels: 108 us -> 94.8 us  [fused_shards(): pl.pallas_call(functools.partial(fused, n, labels, outer_steps, inner_ste...]
where the time goes in v3:
time: 97.9 us; the launch traced here: 97.5 us
  Pallas kernels  96.7 us (99%)
    pallas_call x1, Pallas kernels, fused_shards(): pl.pallas_call(functools.partial(fused, n, labels, outer_steps, inner_ste...  94.8 us

profile of v3, /device:TPU:7, one launch (start us, length us, event | category | flops | bytes accessed | tf_op | source)
XLA Modules:
  0.0 97.5 jit_solution(10943052455134450664)
XLA Ops:
  0.6 94.8 %shard_map.171 = (bf16[2048,256]{1,0:T(8,128)(2,1)S(1)}, bf16[2048,256]{1,0:T(8,128)(2,1)S(1)}, bf16[256,2048]{1,0:T(8,128)(2,1)S(1)}, f32[256,128]{1,0:T(8,128)...) custom-call(bf16[256,2048]{1,0:T(8,128)(2,1)} %cot_hbm.1, ...), custom_call_target="tpu_custom_call" | custom-call | tf_op jit(solution)/shard_map/pallas_call | solution.py:1003
  95.4 1.9 %shard_map.172 = (bf16[2048,256]{1,0:T(8,128)(2,1)}, bf16[2048,256]{1,0:T(8,128)(2,1)}, bf16[256,2048]{1,0:T(8,128)(2,1)}, f32[256,128]{1,0:T(8,128)}, f32[256,1...) custom-call(bf16[2048,256]{1,0:T(8,128)(2,1)S(1)} %get-tuple-element.21.refs_0_, ...), custom_call_target="tpu_custom_call" | custom-call | tf_op jit(solution)/shard_map/pallas_call | solution.py:1063

commit v4 on v3

--- a/solution.py
+++ b/solution.py
@@ -241,6 +241,7 @@
     rows,
     a_send,
     close_send,
+    extra_send,
     w_pair,
     w_down,
     hidden,
@@ -264,6 +265,7 @@
     route_sem,
     raw_sem,
     close_sem,
+    extra_sem,
     a_sem,
     b_sem,
     c_sem,
@@ -449,6 +451,22 @@
         ]
         for j in range(2)
     ]
+    extra_out, extra_in = (
+        [
+            [
+                remote(
+                    extra_send.at[j, i],
+                    rows.at[i, block(place[2 + j]), columns(q_y)],
+                    (extra_sem.at[j, i], b_sem.at[1, i, place[2 + j]]),
+                    flipped(me, 2 + j),
+                    t,
+                )
+                for i in range(2)
+            ]
+            for j in range(2)
+        ]
+        for _ in range(2)
+    )
     to_near, to_opposite, on_opposite, on_near = [], [], [], [[], []]
     for i, ref in enumerate((stream_ref, cot_ref)):
         own = ref.at[:, columns(q)]
@@ -525,7 +543,7 @@
 
     @pl.when(inside == 1)
     def _():
-        for j in range(2):
+        for j in (1, 0):
             close_send[j, 0], close_send[j, 1] = compacted(flipped(me, 2 + j), [columns(q)])[0]
             for i in range(2):
                 close[j][i].start()
@@ -551,7 +569,7 @@
             y_send.at[block(p)], y_got.at[block(p)], (y_sem.at[0, p], y_sem.at[1, p]), me, t_y
         )
 
-    def compact_far(line, i):
+    def compact_far(line, i, direct):
         far = far_route.at[line - 1]
         if i == 0:
             route_in[line - 1].wait_recv()
@@ -571,16 +589,17 @@
                 a[p][i].start()
             else:
                 rows[i, block(p), columns(q)] = part.astype(bf16)
-                b[p][i].start()
+                if 2 * line not in direct:
+                    b[p][i].start()
                 c_near[p][i].start()
 
-    def first_line(i):
+    def first_line(i, direct):
         def go(_):
             to_near[i].wait_recv()
             on_opposite[i].start()
             to_opposite[i].wait_recv()
             on_near[0][i].start()
-            compact_far(1, i)
+            compact_far(1, i, direct)
 
         return go
 
@@ -595,7 +614,7 @@
         def go(_):
             if waits:
                 on_near[line - 2][i].wait_recv()
-            compact_far(line, i)
+            compact_far(line, i, ())
 
         return go
 
@@ -616,19 +635,29 @@
             expert = flipped(me, k)
             pick_ref[dynamic_block(expert), :] = one_hot(slots_of(route, expert))
 
-    def arrive(i):
+    def to_close_more(j):
+        def go(_):
+            extra_send[j, 0], extra_send[j, 1] = compacted(flipped(me, 2 + j), [columns(q_y)])[0]
+            for copy in extra_out[j]:
+                copy.start()
+
+        return go
+
+    def arrive(i, direct):
         def go(p):
             (a[p] or close[0])[i].wait_recv()
-            if labels[p] != 1:
+            if labels[p] not in direct:
                 b[p][i].start()
             c_near[p][i].start()
 
         return go
 
-    def cross(i):
+    def cross(i, direct):
         def go(p):
             if labels[p] == 1:
                 a_extra[p][i].wait_recv()
+            elif labels[p] in direct:
+                extra_in[labels[p] - 2][i].wait_recv()
             else:
                 b[p][i].wait_recv()
             c_far[p][i].start()
@@ -730,12 +759,12 @@
     def all_down(p):
         lax.fori_loop(0, width // step, down, 0)
 
-    def follow(steps, waits):
+    def follow(steps, waits, direct):
         run = dict(
-            a=arrive(0),
-            A=arrive(1),
-            b=cross(0),
-            B=cross(1),
+            a=arrive(0, direct),
+            A=arrive(1, direct),
+            b=cross(0, direct),
+            B=cross(1, direct),
             C=gather,
             E=expert,
             R=reduce_core,
@@ -744,8 +773,10 @@
             G=first_gate_up,
             H=second_gate_up,
             D=all_down,
-            w=first_line(0),
-            W=first_line(1),
+            w=first_line(0, direct),
+            W=first_line(1, direct),
+            U=to_close_more(0),
+            u=to_close_more(1),
             X=to_side,
             Z=to_side_more,
             P=other_picks,
@@ -762,11 +793,11 @@
 
     @pl.when(inside == 0)
     def _():
-        follow(outer_steps, True)
+        follow(outer_steps, True, (1,))
 
     @pl.when(inside == 1)
     def _():
-        follow(inner_steps, False)
+        follow(inner_steps, False, (1, 2, 3))
 
     for p, label in enumerate(labels):
         if label:
@@ -886,7 +917,7 @@
         p = place[label]
         for copy in (a[p] if label != 3 else []) + a_extra[p] + c_near[p] + c_far[p]:
             copy.wait_send()
-        for copy in b[p] if label > 1 else []:
+        for copy in b[p] if label > 3 else []:
             copy.wait_send()
         back_out[p].wait_send()
     for copy in route_out:
@@ -894,7 +925,7 @@
 
     @pl.when(inside == 0)
     def _():
-        for copy in to_near:
+        for copy in to_near + b[place[2]] + b[place[3]] + extra_out[0] + extra_out[1]:
             copy.wait_send()
         route_in[0].wait_recv()
 
@@ -964,14 +995,14 @@
     per = width // n
     labels = [0, 1, 2, 3, 4, 5, 6, 7]
     outer_steps = (
-        "X Z E0 R0 a2 A2 b2 a3 B2 A3 C2 E2 R2 J Y0 V P b3 B3 C3 E3 R3 K Y2 a1 A1 a5 b1 B1 C1 E1"
-        " L A5 b4 B4 C4 E4 R4 a7 M Y3 b5 B5 C5 E5 R5 Y4 A7 R1 b6 B6 C6 E6 R6 Y5 Y1"
-        " b7 B7 C7 E7 R7 Y6 Y7 G H D"
+        "X Z E0 R0 U u a3 A3 a2 b3 A2 B3 C3 E3 R3 Y0 V P a1 A1 b1 B1 J C1 E1 R1 b2 B2 K a5 C2"
+        " E2 A5 b4 B4 C4 L E4 R4 Y3 a7 M b5 B5 C5 E5 R5 A7 Y4 b6 B6 C6 E6 Y5 R6 b7 B7 C7 E7 R7"
+        " R2 Y1 Y6 G H Y7 Y2 D"
     )
     inner_steps = (
-        "E0 R0 w J W K X a3 a5 b2 B2 S L A3 A5 C2 E2 R2 Y0 V P T M Z b4 B4 C4 E4 R4 a7"
-        " b3 B3 C3 E3 R3 Y2 A7 b5 B5 C5 E5 R5 Y4 a1 A1 b6 B6 C6 E6 R6 Y3 b1 B1 C1 E1 R1 Y5"
-        " b7 B7 C7 E7 R7 Y6 Y1 Y7 G H D"
+        "E0 R0 w J W K a5 a3 b4 B4 S L C4 E4 R4 T M X A5 A3 Z Y0 V P b2 B2 C2 E2 R2 a7 Y4 b5"
+        " B5 C5 E5 R5 A7 b6 B6 C6 E6 R6 Y5 Y2 b7 B7 C7 E7 R7 Y6 b3 B3 C3 E3 R3 Y7 a1 A1 b1 B1"
+        " C1 E1 Y3 R1 G Y1 H D"
     )
     vmem = pl.BlockSpec(memory_space=pltpu.VMEM)
     hbm = pl.BlockSpec(memory_space=pltpu.HBM)
@@ -1023,6 +1054,7 @@
             pltpu.VMEM((2, slots, width), bf16),
             pltpu.VMEM((n // 2 + 1, 2, capacity, quarter), bf16),
             pltpu.VMEM((2, 2, capacity, quarter), bf16),
+            pltpu.VMEM((2, 2, capacity, quarter), bf16),
             pltpu.VMEM((width, 2 * units), bf16),
             pltpu.VMEM((units, width), bf16),
             pltpu.VMEM((slots, units), bf16),
@@ -1045,6 +1077,7 @@
             dma((12,)),
             dma((2, 3)),
             dma((8, 2)),
+            dma((2, 2)),
             dma((2, 2)),
             dma((2, 2, n)),
             dma((2, 2, n)),

time: 97.9 us -> 96.8 us (0.989)
  no operation moved by 1% of the time
where the time goes in v4:
time: 96.8 us; the launch traced here: 96.6 us
  Pallas kernels  95.8 us (99%)
    pallas_call x1, Pallas kernels, fused_shards(): pl.pallas_call(functools.partial(fused, n, labels, outer_steps, inner_ste...  93.9 us

profile of v4, /device:TPU:7, one launch (start us, length us, event | category | flops | bytes accessed | tf_op | source)
XLA Modules:
  0.0 96.6 jit_solution(17224644088499195722)
XLA Ops:
  0.6 93.9 %shard_map.171 = (bf16[2048,256]{1,0:T(8,128)(2,1)S(1)}, bf16[2048,256]{1,0:T(8,128)(2,1)S(1)}, bf16[256,2048]{1,0:T(8,128)(2,1)S(1)}, f32[256,128]{1,0:T(8,128)...) custom-call(bf16[256,2048]{1,0:T(8,128)(2,1)} %cot_hbm.1, ...), custom_call_target="tpu_custom_call" | custom-call | tf_op jit(solution)/shard_map/pallas_call | solution.py:1034
  94.5 1.9 %shard_map.172 = (bf16[2048,256]{1,0:T(8,128)(2,1)}, bf16[2048,256]{1,0:T(8,128)(2,1)}, bf16[256,2048]{1,0:T(8,128)(2,1)}, f32[256,128]{1,0:T(8,128)}, f32[256,1...) custom-call(bf16[2048,256]{1,0:T(8,128)(2,1)S(1)} %get-tuple-element.21.refs_0_, ...), custom_call_target="tpu_custom_call" | custom-call | tf_op jit(solution)/shard_map/pallas_call | solution.py:1096

commit v5 on v4

--- a/solution.py
+++ b/solution.py
@@ -262,10 +262,9 @@
     conv_out,
     mixer_out,
     load_sem,
+    out_sem,
     route_sem,
     raw_sem,
-    close_sem,
-    extra_sem,
     a_sem,
     b_sem,
     c_sem,
@@ -402,7 +401,7 @@
                     remote(
                         a_send.at[label // 2, i],
                         mine,
-                        (a_sem.at[0, i, p], a_sem.at[1, i, p]),
+                        (out_sem.at[4], a_sem.at[i, p]),
                         across_x,
                         t,
                     )
@@ -412,29 +411,29 @@
                     remote(
                         a_send.at[sp_devices // 2, i],
                         theirs,
-                        (a_sem.at[0, i, 0], a_sem.at[1, i, 0]),
+                        (out_sem.at[4], a_sem.at[i, 0]),
                         across_x,
                         t,
                     )
                 )
-            b[p].append(remote(mine, mine, (b_sem.at[0, i, p], b_sem.at[1, i, p]), me, t_y))
+            b[p].append(remote(mine, mine, (out_sem.at[5], b_sem.at[i, p]), me, t_y))
             c_near[p].append(
-                remote(mine, mine, (c_sem.at[0, i, p], c_sem.at[1, i, p]), me, t_core)
+                remote(mine, mine, (out_sem.at[6], c_sem.at[p]), me, t_core)
             )
             c_far[p].append(
-                remote(theirs, theirs, (c_sem.at[2, i, p], c_sem.at[3, i, p]), me, t_core)
+                remote(theirs, theirs, (out_sem.at[6], c_sem.at[p]), me, t_core)
             )
         back_out[p] = remote(
             back_send.at[block(p)],
             back_got.at[dynamic_block(me)],
-            (back_sem.at[0, p], back_sem.at[1, me]),
+            (out_sem.at[9], back_sem.at[me]),
             partner,
             t,
         )
         back_in[p] = remote(
             back_send.at[block(p)],
             back_got.at[dynamic_block(partner)],
-            (back_sem.at[0, p], back_sem.at[1, partner]),
+            (out_sem.at[9], back_sem.at[partner]),
             partner,
             t,
         )
@@ -443,7 +442,7 @@
             remote(
                 close_send.at[j, i],
                 rows.at[i, block(place[2 + j]), columns(q)],
-                (close_sem.at[j, i], a_sem.at[1, i, place[2 + j]]),
+                (out_sem.at[2], a_sem.at[i, place[2 + j]]),
                 flipped(me, 2 + j),
                 t,
             )
@@ -457,7 +456,7 @@
                 remote(
                     extra_send.at[j, i],
                     rows.at[i, block(place[2 + j]), columns(q_y)],
-                    (extra_sem.at[j, i], b_sem.at[1, i, place[2 + j]]),
+                    (out_sem.at[3], b_sem.at[i, place[2 + j]]),
                     flipped(me, 2 + j),
                     t,
                 )
@@ -471,52 +470,52 @@
     for i, ref in enumerate((stream_ref, cot_ref)):
         own = ref.at[:, columns(q)]
         to_near.append(
-            remote(own, raw.at[0, i], (raw_sem.at[0, i], raw_sem.at[5, i]), near, t)
+            remote(own, raw.at[0, i], (out_sem.at[1], raw_sem.at[0, i]), near, t)
         )
         to_opposite.append(
-            remote(own, raw.at[1, i], (raw_sem.at[1, i], raw_sem.at[6, i]), opposite, t)
+            remote(own, raw.at[1, i], (out_sem.at[1], raw_sem.at[1, i]), opposite, t)
         )
         on_opposite.append(
-            remote(raw.at[0, i], raw.at[2, i], (raw_sem.at[2, i], raw_sem.at[7, i]), opposite, t)
+            remote(raw.at[0, i], raw.at[2, i], (out_sem.at[1], raw_sem.at[2, i]), opposite, t)
         )
         for j in range(2):
             on_near[j].append(
                 remote(
                     raw.at[1 + j, i],
                     raw.at[1 + j, i],
-                    (raw_sem.at[3 + j, i], raw_sem.at[6 + j, i]),
+                    (out_sem.at[1], raw_sem.at[1 + j, i]),
                     near,
                     t,
                 )
             )
     as_far = 2 - inside
     route_out = [
-        remote(route, far_route.at[0], (route_sem.at[0, 0], route_sem.at[1, 0]), near, t)
+        remote(route, far_route.at[0], (out_sem.at[0], route_sem.at[0]), near, t)
     ] + [
         remote(
             route,
             far_route.at[as_far],
-            (route_sem.at[0, j], route_sem.at[1, as_far]),
+            (out_sem.at[0], route_sem.at[as_far]),
             flipped(me, 2 + 2 * j),
             t,
         )
         for j in (1, 2)
     ]
     route_in = [
-        remote(route, far_route.at[j], (route_sem.at[0, j], route_sem.at[1, j]), near, t)
+        remote(route, far_route.at[j], (out_sem.at[0], route_sem.at[j]), near, t)
         for j in range(3)
     ]
     to_next = remote(
         before.at[pl.ds(tokens, 8)],
         before.at[pl.ds(0, 8)],
-        (conv_sem.at[0], conv_sem.at[1]),
+        (out_sem.at[12], conv_sem.at[0]),
         me + 1,
         t,
     )
     to_previous = remote(
         after.at[pl.ds(0, 8)],
         after.at[pl.ds(tokens, 8)],
-        (conv_sem.at[2], conv_sem.at[3]),
+        (out_sem.at[13], conv_sem.at[1]),
         me - 1,
         t,
     )
@@ -559,14 +558,14 @@
             remote(
                 core_send.at[i, block(p)],
                 core_got.at[i, block(p)],
-                (core_sem.at[0, i, p], core_sem.at[1, i, p]),
+                (out_sem.at[7], core_sem.at[i, p]),
                 me,
                 t_core,
             )
             for i in range(2)
         ]
         y_hop[p] = remote(
-            y_send.at[block(p)], y_got.at[block(p)], (y_sem.at[0, p], y_sem.at[1, p]), me, t_y
+            y_send.at[block(p)], y_got.at[block(p)], (out_sem.at[8], y_sem.at[p]), me, t_y
         )
 
     def compact_far(line, i, direct):
@@ -665,9 +664,8 @@
         return go
 
     def gather(p):
-        for i in range(2):
-            c_near[p][i].wait_recv()
-            c_far[p][i].wait_recv()
+        four = core_got.at[:, pl.ds(0, 2 * capacity)]
+        remote(four, four, (out_sem.at[6], c_sem.at[p]), me, t_core).wait_recv()
 
     def expert(p):
         span = block(p)
@@ -813,12 +811,11 @@
         part, part_y = stream_grad.at[:, piece_of(q, i)], stream_grad.at[:, piece_of(q_y, i)]
         gathers.append(
             [
-                remote(part, part, (gather_sem.at[0, 0, i], gather_sem.at[1, 0, i]), me, t_y),
-                remote(part, part, (gather_sem.at[0, 1, i], gather_sem.at[1, 1, i]), me, t_core),
-                remote(part_y, part_y, (gather_sem.at[0, 2, i], gather_sem.at[1, 2, i]), me, t_core),
+                remote(part, part, (out_sem.at[10], gather_sem.at[0, i]), me, t_y),
+                remote(part, part, (out_sem.at[10], gather_sem.at[1, i]), me, t_core),
+                remote(part_y, part_y, (out_sem.at[10], gather_sem.at[2, i]), me, t_core),
             ]
         )
-    sends = []
 
     def project(j, index, i):
         piece = stream_grad[:, piece_of(index, i)]
@@ -829,7 +826,7 @@
         send = remote(
             proj_send.at[j * share + i],
             proj_got.at[me],
-            (proj_sem.at[0, j * share + i], proj_sem.at[1, me]),
+            (out_sem.at[11], proj_sem.at[me]),
             owner,
             t,
         )
@@ -842,7 +839,6 @@
         def _():
             proj_got[me] = proj_send[j * share + i]
 
-        sends.append((owner, send))
         return jnp.dot(piece, out_proj_ref[piece_of(index, i), :], preferred_element_type=f32)
 
     for i in range(share):
@@ -904,7 +900,7 @@
             remote(
                 proj_send.at[0],
                 proj_got.at[source],
-                (proj_sem.at[0, 0], proj_sem.at[1, source]),
+                (out_sem.at[11], proj_sem.at[source]),
                 source,
                 t,
             ).wait_recv()
@@ -913,41 +909,32 @@
         total = total + proj_got[s].astype(f32)
     grad_proj_ref[...] = total
 
-    for label in others:
-        p = place[label]
-        for copy in (a[p] if label != 3 else []) + a_extra[p] + c_near[p] + c_far[p]:
-            copy.wait_send()
-        for copy in b[p] if label > 3 else []:
-            copy.wait_send()
-        back_out[p].wait_send()
-    for copy in route_out:
-        copy.wait_send()
+    def drained(kind, ref):
+        remote(ref, ref, (out_sem.at[kind], conv_sem.at[0]), me, t_core).wait_send()
+
+    pieces = sp_devices - 1
+    drained(0, far_route)
+    drained(6, rows.at[:, pl.ds(0, pieces * capacity), pl.ds(0, 2 * quarter)])
+    drained(7, core_send)
+    drained(8, y_send)
+    drained(9, back_send.at[pl.ds(0, pieces * capacity)])
+    drained(10, stream_grad.at[:, pl.ds(0, 3 * quarter)])
+    drained(11, proj_send.at[pl.ds(0, pieces)])
 
     @pl.when(inside == 0)
     def _():
-        for copy in to_near + b[place[2]] + b[place[3]] + extra_out[0] + extra_out[1]:
-            copy.wait_send()
+        drained(1, raw.at[0])
+        drained(3, extra_send)
+        drained(4, a_send.at[pl.ds(0, sp_devices // 2)])
+        drained(5, rows.at[:, pl.ds(0, (pieces - 1) * capacity), pl.ds(0, quarter)])
         route_in[0].wait_recv()
 
     @pl.when(inside == 1)
     def _():
-        for copy in a[place[3]] + to_opposite + on_opposite + on_near[0] + on_near[1]:
-            copy.wait_send()
-        for copy in close[0] + close[1]:
-            copy.wait_send()
-
-    for p in range(len(labels)):
-        core[p][0].wait_send()
-        core[p][1].wait_send()
-        y_hop[p].wait_send()
-    for copies in gathers:
-        for copy in copies:
-            copy.wait_send()
-    for owner, send in sends:
-
-        @pl.when(owner != me)
-        def _():
-            send.wait_send()
+        drained(1, rows.at[:, :, pl.ds(0, quarter)])
+        drained(2, close_send)
+        drained(4, a_send)
+        drained(5, rows.at[:, pl.ds(0, (pieces - 3) * capacity), pl.ds(0, quarter)])
 
     @pl.when(me < sp_devices - 1)
     def _():
@@ -1075,19 +1062,18 @@
             pltpu.VMEM((tokens, channels), f32),
             pltpu.VMEM((tokens, channels), bf16),
             dma((12,)),
-            dma((2, 3)),
-            dma((8, 2)),
-            dma((2, 2)),
-            dma((2, 2)),
-            dma((2, 2, n)),
-            dma((2, 2, n)),
-            dma((4, 2, n)),
-            dma((2, 2, n)),
+            dma((14,)),
+            dma((3,)),
+            dma((3, 2)),
             dma((2, n)),
             dma((2, n)),
-            dma((2, 3, quarter // per)),
+            dma((n,)),
             dma((2, n)),
-            dma((4,)),
+            dma((n,)),
+            dma((n,)),
+            dma((3, quarter // per)),
+            dma((n,)),
+            dma((2,)),
         ],
         compiler_params=pltpu.CompilerParams(
             collective_id=0, has_side_effects=True, vmem_limit_bytes=48 * 1024 * 1024

time: 96.8 us -> 95.4 us (0.986)
  Pallas kernels: 95.8 us -> 94.3 us
    pallas_call x1, Pallas kernels: 93.9 us -> 92.5 us  [fused_shards(): pl.pallas_call(functools.partial(fused, n, labels, outer_steps, inner_ste...]
where the time goes in v5:
time: 95.4 us; the launch traced here: 95.2 us
  Pallas kernels  94.3 us (99%)
    pallas_call x1, Pallas kernels, fused_shards(): pl.pallas_call(functools.partial(fused, n, labels, outer_steps, inner_ste...  92.5 us

profile of v5, /device:TPU:7, one launch (start us, length us, event | category | flops | bytes accessed | tf_op | source)
XLA Modules:
  0.0 95.2 jit_solution(4958107213770254947)
XLA Ops:
  0.6 92.5 %shard_map.171 = (bf16[2048,256]{1,0:T(8,128)(2,1)S(1)}, bf16[2048,256]{1,0:T(8,128)(2,1)S(1)}, bf16[256,2048]{1,0:T(8,128)(2,1)S(1)}, f32[256,128]{1,0:T(8,128)...) custom-call(bf16[256,2048]{1,0:T(8,128)(2,1)} %cot_hbm.1, ...), custom_call_target="tpu_custom_call" | custom-call | tf_op jit(solution)/shard_map/pallas_call | solution.py:1021
  93.1 1.9 %shard_map.172 = (bf16[2048,256]{1,0:T(8,128)(2,1)}, bf16[2048,256]{1,0:T(8,128)(2,1)}, bf16[256,2048]{1,0:T(8,128)(2,1)}, f32[256,128]{1,0:T(8,128)}, f32[256,1...) custom-call(bf16[2048,256]{1,0:T(8,128)(2,1)S(1)} %get-tuple-element.21.refs_0_, ...), custom_call_target="tpu_custom_call" | custom-call | tf_op jit(solution)/shard_map/pallas_call | solution.py:1082

commit v6 on v5

--- a/solution.py
+++ b/solution.py
@@ -802,12 +802,14 @@
             with scope(f"back{label}"):
                 back_in[p].wait_recv()
     share = quarter // per
+    cut = per // 2
+    cuts = quarter // cut
 
     def piece_of(index, i):
-        return pl.ds(pl.multiple_of(index * quarter + i * per, per), per)
+        return pl.ds(pl.multiple_of(index * quarter + i * cut, cut), cut)
 
     gathers = []
-    for i in range(share):
+    for i in range(cuts):
         part, part_y = stream_grad.at[:, piece_of(q, i)], stream_grad.at[:, piece_of(q_y, i)]
         gathers.append(
             [
@@ -819,16 +821,13 @@
 
     def project(j, index, i):
         piece = stream_grad[:, piece_of(index, i)]
-        proj_send[j * share + i] = lax.dot_general(
+        proj_send[j * cuts + i] = lax.dot_general(
             piece, mixer_out[...], over_rows, preferred_element_type=f32
         ).astype(bf16)
-        owner = index * share + i
+        owner = index * share + i // 2
+        landing = proj_got.at[me, pl.ds(i % 2 * cut, cut)]
         send = remote(
-            proj_send.at[j * share + i],
-            proj_got.at[me],
-            (out_sem.at[11], proj_sem.at[me]),
-            owner,
-            t,
+            proj_send.at[j * cuts + i], landing, (out_sem.at[11], proj_sem.at[me]), owner, t
         )
 
         @pl.when(owner != me)
@@ -837,12 +836,12 @@
 
         @pl.when(owner == me)
         def _():
-            proj_got[me] = proj_send[j * share + i]
+            landing[...] = proj_send[j * cuts + i]
 
         return jnp.dot(piece, out_proj_ref[piece_of(index, i), :], preferred_element_type=f32)
 
     for i in range(share):
-        at = piece_of(q, i)
+        at = pl.ds(pl.multiple_of(q * quarter + i * per, per), per)
         moe_grad = lax.dot_general(
             pick_ref[...],
             back_got[:, pl.ds(i * per, per)],
@@ -850,16 +849,17 @@
             preferred_element_type=f32,
         )
         stream_grad[:, at] = (cot_ref[:, at].astype(f32) + moe_grad).astype(bf16)
-        gathers[i][0].start()
-        gathers[i][1].start()
+        for k in (2 * i, 2 * i + 1):
+            gathers[k][0].start()
+            gathers[k][1].start()
     d_mixer = project(0, q, 0)
-    for i in range(1, share):
+    for i in range(1, cuts):
         d_mixer = d_mixer + project(0, q, i)
-    for i in range(share):
+    for i in range(cuts):
         with scope(f"g1{i}"):
             gathers[i][1].wait_recv()
         d_mixer = d_mixer + project(1, q_core, i)
-    for i in range(share):
+    for i in range(cuts):
         with scope(f"g0{i}"):
             gathers[i][0].wait_recv()
         gathers[i][2].start()
@@ -898,7 +898,7 @@
         source = flipped(me, k)
         with scope(f"pw{k}"):
             remote(
-                proj_send.at[0],
+                proj_got.at[source],
                 proj_got.at[source],
                 (out_sem.at[11], proj_sem.at[source]),
                 source,
@@ -919,7 +919,7 @@
     drained(8, y_send)
     drained(9, back_send.at[pl.ds(0, pieces * capacity)])
     drained(10, stream_grad.at[:, pl.ds(0, 3 * quarter)])
-    drained(11, proj_send.at[pl.ds(0, pieces)])
+    drained(11, proj_send.at[pl.ds(0, 2 * pieces)])
 
     @pl.when(inside == 0)
     def _():
@@ -1055,7 +1055,7 @@
             pltpu.VMEM((slots, quarter), bf16),
             pltpu.VMEM((slots, quarter), bf16),
             pltpu.VMEM((tokens, width), bf16),
-            pltpu.VMEM((n, per, channels), bf16),
+            pltpu.VMEM((2 * n, per // 2, channels), bf16),
             pltpu.VMEM((n, per, channels), bf16),
             pltpu.VMEM((tokens + 8, channels), f32),
             pltpu.VMEM((tokens + 8, channels), f32),
@@ -1071,7 +1071,7 @@
             dma((2, n)),
             dma((n,)),
             dma((n,)),
-            dma((3, quarter // per)),
+            dma((3, 2 * quarter // per)),
             dma((n,)),
             dma((2,)),
         ],

time: 95.4 us -> 94.2 us (0.987)
  Pallas kernels: 94.3 us -> 93.2 us
    pallas_call x1, Pallas kernels: 92.5 us -> 91.3 us  [fused_shards(): pl.pallas_call(functools.partial(fused, n, labels, outer_steps, inner_ste...]
where the time goes in v6:
time: 94.2 us; the launch traced here: 94.1 us
  Pallas kernels  93.2 us (99%)
    pallas_call x1, Pallas kernels, fused_shards(): pl.pallas_call(functools.partial(fused, n, labels, outer_steps, inner_ste...  91.3 us
    pallas_call x1, Pallas kernels, fused_shards(): pl.pallas_call(written, out_shape=[jax.ShapeDtypeStruct(*shape) for shape...  1.88 us

profile of v6, /device:TPU:7, one launch (start us, length us, event | category | flops | bytes accessed | tf_op | source)
XLA Modules:
  0.0 94.1 jit_solution(13462654994337872928)
XLA Ops:
  0.6 91.3 %shard_map.171 = (bf16[2048,256]{1,0:T(8,128)(2,1)S(1)}, bf16[2048,256]{1,0:T(8,128)(2,1)S(1)}, bf16[256,2048]{1,0:T(8,128)(2,1)S(1)}, f32[256,128]{1,0:T(8,128)...) custom-call(bf16[256,2048]{1,0:T(8,128)(2,1)} %cot_hbm.1, ...), custom_call_target="tpu_custom_call" | custom-call | tf_op jit(solution)/shard_map/pallas_call | solution.py:1021
  92.0 1.9 %shard_map.172 = (bf16[2048,256]{1,0:T(8,128)(2,1)}, bf16[2048,256]{1,0:T(8,128)(2,1)}, bf16[256,2048]{1,0:T(8,128)(2,1)}, f32[256,128]{1,0:T(8,128)}, f32[256,1...) custom-call(bf16[2048,256]{1,0:T(8,128)(2,1)S(1)} %get-tuple-element.21.refs_0_, ...), custom_call_target="tpu_custom_call" | custom-call | tf_op jit(solution)/shard_map/pallas_call | solution.py:1082
